TPU v7x, 512 devices: a whole 4x4x16 slice. The times are simulated.
512 devices in a mesh: sp: 128 (over z, x, core), tp: 4 (over y).
Axes of the slice: x: 4, y: 4, z: 16, core: 2. Of those that a mesh axis runs over, the one named last changes fastest.
Arguments:
- inputs: bfloat16 [4, 16384, 1024], P(None, 'sp'), may hold values from -6 to 6
- norm_gain: float32 [1024], replicated, may hold values from 0.1 to 1.9
- query_weight: bfloat16 [1024, 3, 8, 64], P('sp', None, 'tp'), may hold values from -0.1875 to 0.1875
- key_weight: bfloat16 [1024, 3, 8, 64], P('sp', None, 'tp'), may hold values from -0.1875 to 0.1875
- value_weight: bfloat16 [1024, 3, 8, 64], P('sp', None, 'tp'), may hold values from -0.1875 to 0.1875
- query_gain: float32 [3, 64], replicated, may hold values from 0.1 to 1.9
- key_gain: float32 [3, 64], replicated, may hold values from 0.1 to 1.9
- out_weight: bfloat16 [8, 64, 1024], P('tp', None, 'sp'), may hold values from -0.75 to 0.75
Outputs:
- mixed: bfloat16 [4, 16384, 1024], P(None, 'sp', 'tp')
All inputs are finite; a program needn't handle non-finite values.
Results may differ from a plain program's by a relative error of at most 0.02.
Values may be sent and summed in bfloat16 or wider, within the bound.
A program may use at most 64 MiB of HBM per device.

v0:
```python
import functools
import math

import jax
import jax.numpy as jnp
from jax import lax
from jax.experimental import pallas as pl
from jax.experimental.pallas import tpu as pltpu
from jax.sharding import PartitionSpec as P

GAPS = ((1, 32), (4, 32), (16, 16))
EPS = 1e-06
NEG = -1e30
MESH = pl.DeviceIdType.MESH


def halo_plan(length):
    plan = []
    for group, (dilation, half) in enumerate(GAPS):
        reach = dilation * half
        for distance in range(1, -(-reach // length) + 1):
            plan.append((group, distance, min(length, reach - (distance - 1) * length)))
    return sorted(plan, key=lambda item: item[1])


def layer_kernel(
    n, tp, batch, length, heads, width, x_ref, gain_ref, wa_ref, wb_ref, qg_ref, kg_ref, out_ref,
    abuf, bbuf, win0, win1, win2, qn, bias, sums, totals, parts, got, halves, others,
    near_send, near_recv, rs_send, rs_recv, ring_send, ring_recv, halo_send, halo_recv,
):
    me = lax.axis_index("sp")
    mine = lax.axis_index("tp")
    groups = len(GAPS)
    lanes = heads * width
    rows = batch * length
    half_n = n // 2

    def ring_to_sp(p):
        return jnp.where(p < half_n, 2 * p, 2 * (n - 1 - p) + 1)

    place = jnp.where(me % 2 == 0, me // 2, n - 1 - me // 2)
    forward = ring_to_sp((place + 1) % n)
    backward = ring_to_sp((place + n - 1) % n)
    bufs = (abuf, bbuf)
    firsts = (wa_ref, wb_ref)

    def hop(chunk, way, step):
        owner = ring_to_sp((place + (n - (step - 1) if way == 0 else step - 1)) % n)
        buf = bufs[chunk]
        columns = buf.shape[2]
        cut = pl.ds(0, columns)
        if step == half_n and n % 2 == 0:
            middle = (columns // 2 + 127) // 128 * 128
            cut = pl.ds(0, middle) if way == 0 else pl.ds(middle, columns - middle)
        src = firsts[chunk].at[:, cut] if step == 1 else buf.at[owner, :, cut]
        return pltpu.make_async_remote_copy(
            src_ref=src,
            dst_ref=buf.at[owner, :, cut],
            send_sem=ring_send.at[chunk, way, step - 1],
            recv_sem=ring_recv.at[chunk, way, step - 1],
            device_id={"sp": forward if way == 0 else backward},
            device_id_type=MESH,
        )

    barrier = pltpu.get_barrier_semaphore()

    def greet(target):
        pl.semaphore_signal(barrier, inc=1, device_id=target, device_id_type=MESH)

    greet({"sp": forward})
    greet({"sp": backward})
    greet({"tp": mine + 1 - 2 * (mine % 2)})
    for shift in range(1, tp // 2):
        greet({"tp": (mine + 2 * shift) % tp})
    plan = halo_plan(length)
    for distance in sorted({item[1] for item in plan}):

        @pl.when(me + distance < n)
        def _(distance=distance):
            greet({"sp": me + distance})

        @pl.when(me >= distance)
        def _(distance=distance):
            greet({"sp": me - distance})

    count = 2 + tp // 2
    for distance in sorted({item[1] for item in plan}):
        count = count + jnp.where(me + distance < n, 1, 0) + jnp.where(me >= distance, 1, 0)
    pl.semaphore_wait(barrier, count)

    for chunk in range(2):
        for way in range(2):
            hop(chunk, way, 1).start()
    for chunk in range(2):
        bufs[chunk][me] = firsts[chunk][...]

    flat = x_ref[...].reshape(rows, -1).astype(jnp.float32)
    scale = lax.rsqrt(jnp.mean(flat * flat, axis=-1, keepdims=True) + EPS)
    normed = (flat * scale * gain_ref[...]).astype(jnp.bfloat16)

    slopes = []
    for head in range(heads):
        power = -8.0 * (mine * heads + head + 1).astype(jnp.float32) / (heads * tp)
        slopes.append(jnp.exp2(jnp.full((8, 128), power, jnp.float32))[:1, :1])
    widths = [length + 2 * d * h for d, h in GAPS]
    starts = [sum(widths[:g]) for g in range(groups)]
    for group, (dilation, half) in enumerate(GAPS):
        reach = dilation * half
        shape = (length, widths[group])
        key = lax.broadcasted_iota(jnp.int32, shape, 1) - reach
        offset = jnp.abs(key - lax.broadcasted_iota(jnp.int32, shape, 0))
        at = key + me * length
        allowed = (offset <= reach) & (at >= 0) & (at < n * length) & ((offset & (dilation - 1)) == 0)
        distance = offset.astype(jnp.float32) / float(reach)
        for head in range(heads):
            value = jnp.where(allowed, -slopes[head] * distance, NEG)
            bias[head, :, starts[group] : starts[group] + widths[group]] = value

    wins = (win0, win1, win2)
    for group, distance, count in plan:
        reach = GAPS[group][0] * GAPS[group][1]
        low = reach - (distance - 1) * length - count
        high = reach + distance * length
        blank = jnp.zeros((batch, count, 2 * lanes), jnp.bfloat16)

        @pl.when(me < distance)
        def _(group=group, low=low, count=count, blank=blank):
            wins[group][:, low : low + count, :] = blank

        @pl.when(me + distance >= n)
        def _(group=group, high=high, count=count, blank=blank):
            wins[group][:, high : high + count, :] = blank

    def finish_ring(chunk):
        for way in range(2):
            hop(chunk, way, half_n).wait_recv()

    def advance(chunk, step):
        if 2 <= step <= half_n:
            for way in range(2):
                hop(chunk, way, step - 1).wait_recv()
                hop(chunk, way, step).start()

    for step in range(2, half_n + 1):
        advance(0, step)
        advance(1, step - 1)

    row_head = lax.broadcasted_iota(jnp.int32, (lanes, lanes), 0) // width
    column_head = lax.broadcasted_iota(jnp.int32, (lanes, lanes), 1) // width
    same_head = jnp.where(row_head == column_head, 1.0 / width, 0.0)

    def repeated(ref, group):
        return jnp.concatenate([ref[group : group + 1, :]] * heads, axis=1)

    def head_norm(block, gain):
        values = block.astype(jnp.bfloat16).astype(jnp.float32)
        mean = jnp.dot(
            values * values, same_head, precision=lax.Precision.HIGHEST, preferred_element_type=jnp.float32
        )
        return values * lax.rsqrt(mean + EPS) * gain

    finish_ring(0)
    depth = abuf.shape[0] * abuf.shape[1]
    def halo(index, up):
        group, distance, count = plan[index]
        reach = GAPS[group][0] * GAPS[group][1]
        win = wins[group]
        if up:
            src = win.at[:, pl.ds(reach + length - count, count), :]
            dst = win.at[:, pl.ds(reach - (distance - 1) * length - count, count), :]
            target = (me + distance) % n
        else:
            src = win.at[:, pl.ds(reach, count), :]
            dst = win.at[:, pl.ds(reach + distance * length, count), :]
            target = (me + n - distance) % n
        side = 0 if up else 1
        return pltpu.make_async_remote_copy(
            src_ref=src,
            dst_ref=dst,
            send_sem=halo_send.at[side, index],
            recv_sem=halo_recv.at[side, index],
            device_id={"sp": target},
            device_id_type=MESH,
        )

    def each_halo(method_up, method_down, inward, only=None):
        for index, (group, distance, count) in enumerate(plan):
            if only is not None and group != only:
                continue
            above = me + distance < n
            below = me >= distance

            @pl.when(below if inward else above)
            def _(index=index):
                method_up(halo(index, True))

            @pl.when(above if inward else below)
            def _(index=index):
                method_down(halo(index, False))

    for group in reversed(range(groups)):
        reach = GAPS[group][0] * GAPS[group][1]
        low = 2 * lanes * group
        weights = abuf[:, :, low : low + 2 * lanes].reshape(depth, 2 * lanes)
        key_values = jnp.dot(normed, weights, preferred_element_type=jnp.float32)
        keys = head_norm(key_values[:, :lanes], repeated(kg_ref, group))
        values = key_values[:, lanes:]
        wins[group][:, reach : reach + length, :lanes] = keys.astype(jnp.bfloat16).reshape(batch, length, lanes)
        wins[group][:, reach : reach + length, lanes:] = values.astype(jnp.bfloat16).reshape(batch, length, lanes)
        if group == groups - 1:
            advance(1, half_n)
        each_halo(lambda c: c.start(), lambda c: c.start(), False, group)

    finish_ring(1)
    factor = 1.0 / math.sqrt(width)
    weights = bbuf[:, :, : groups * lanes].reshape(depth, groups * lanes)
    queries = jnp.dot(normed, weights, preferred_element_type=jnp.float32)
    for group in range(groups):
        block = head_norm(queries[:, lanes * group : lanes * (group + 1)], repeated(qg_ref, group) * factor)
        qn[group] = block.astype(jnp.bfloat16).reshape(batch, length, lanes)

    lane_head = lax.broadcasted_iota(jnp.int32, (length, lanes), 1) // width
    span = depth // tp
    pairs = tp // 2
    parity = mine % 2
    level = mine // 2

    def attend(group, b):
        total = jnp.zeros((length, lanes), jnp.float32)
        summed = jnp.zeros((length, lanes), jnp.float32)
        query_all = qn[group, b]
        for head in range(heads):
            here = lane_head == head
            query = jnp.where(here, query_all, jnp.zeros_like(query_all))
            scores = lax.dot_general(
                query, wins[group][b, :, :lanes], (((1,), (1,)), ((), ())), preferred_element_type=jnp.float32
            )
            grown = jnp.exp(scores + bias[head, :, starts[group] : starts[group] + widths[group]])
            total = jnp.where(here, jnp.sum(grown, axis=-1, keepdims=True), total)
            result = jnp.dot(
                grown.astype(jnp.bfloat16), wins[group][b, :, lanes:], preferred_element_type=jnp.float32
            )
            summed = jnp.where(here, result, summed)
        return summed, total

    def to_partner(b):
        return pltpu.make_async_remote_copy(
            src_ref=parts.at[b, 1 - parity],
            dst_ref=got.at[b],
            send_sem=near_send.at[b],
            recv_sem=near_recv.at[b],
            device_id={"tp": mine + 1 - 2 * parity},
            device_id_type=MESH,
        )

    def to_level(b, shift):
        target = (level + shift) % pairs
        return pltpu.make_async_remote_copy(
            src_ref=halves.at[b, target],
            dst_ref=others.at[b, shift - 1],
            send_sem=rs_send.at[b, shift - 1],
            recv_sem=rs_recv.at[b, shift - 1],
            device_id={"tp": 2 * target + parity},
            device_id_type=MESH,
        )

    def pass_on(b):
        to_partner(b).wait_recv()
        halves[b] = (parts[b, parity].astype(jnp.float32) + got[b].astype(jnp.float32)).astype(jnp.bfloat16)
        for shift in range(1, pairs):
            to_level(b, shift).start()

    outs = bbuf[:, :, groups * lanes :].reshape(depth, lanes)

    def first_groups(group):
        def step(b, carry):
            summed, total = attend(group, b)
            if group == groups - 1:
                sums[b], totals[b] = summed, total
            else:
                sums[b] += summed
                totals[b] += total
            return carry

        return step

    def last_group(b, carry):
        summed, total = attend(0, b)
        merged = ((sums[b] + summed) / (totals[b] + total)).astype(jnp.bfloat16)
        term = lax.dot_general(merged, outs, (((1,), (1,)), ((), ())), preferred_element_type=jnp.float32)
        for block in range(tp):
            parts[b, block % 2, block // 2] = term[:, block * span : (block + 1) * span].astype(jnp.bfloat16)
        to_partner(b).start()

        @pl.when(b >= 1)
        def _():
            pass_on(b - 1)

        return carry

    for group in reversed(range(groups)):
        each_halo(lambda c: c.wait_recv(), lambda c: c.wait_recv(), True, group)
        lax.fori_loop(0, batch, last_group if group == 0 else first_groups(group), 0)
    pass_on(batch - 1)

    def finish(b, carry):
        final = parts[b, parity, level].astype(jnp.float32) + got[b, level].astype(jnp.float32)
        for shift in range(1, pairs):
            to_level(b, shift).wait_recv()
            final = final + others[b, shift - 1].astype(jnp.float32)
        out_ref[b] = final.astype(jnp.bfloat16)
        for shift in range(1, pairs):
            to_level(b, shift).wait_send()
        to_partner(b).wait_send()
        return carry

    lax.fori_loop(0, batch, finish, 0)
    for step in range(1, half_n + 1):
        for chunk in range(2):
            for way in range(2):
                hop(chunk, way, step).wait_send()
    each_halo(lambda c: c.wait_send(), lambda c: c.wait_send(), False)


def body(n, tp, inputs, norm_gain, query_weight, key_weight, value_weight, query_gain, key_gain, out_weight):
    batch, length, model = inputs.shape
    share, groups, heads, width = query_weight.shape
    lanes = heads * width
    key_values = jnp.stack(
        [key_weight.reshape(share, groups, lanes), value_weight.reshape(share, groups, lanes)], axis=2
    ).reshape(share, groups * 2 * lanes)
    outs = out_weight.reshape(lanes, -1).T
    rest = jnp.concatenate([query_weight.reshape(share, groups * lanes), outs], axis=1)
    total = sum(length + 2 * d * h for d, h in GAPS)
    windows = [pltpu.VMEM((batch, length + 2 * d * h, 2 * lanes), jnp.bfloat16) for d, h in GAPS]
    plan = halo_plan(length)
    vmem = pl.BlockSpec(memory_space=pltpu.VMEM)
    span = model // tp
    return pl.pallas_call(
        functools.partial(layer_kernel, n, tp, batch, length, heads, width),
        out_shape=jax.ShapeDtypeStruct((batch, length, span), jnp.bfloat16),
        in_specs=[vmem] * 6,
        out_specs=vmem,
        scratch_shapes=[
            pltpu.VMEM((n, share, key_values.shape[1]), jnp.bfloat16),
            pltpu.VMEM((n, share, rest.shape[1]), jnp.bfloat16),
            *windows,
            pltpu.VMEM((groups, batch, length, lanes), jnp.bfloat16),
            pltpu.VMEM((heads, length, total), jnp.float32),
            pltpu.VMEM((batch, length, lanes), jnp.float32),
            pltpu.VMEM((batch, length, lanes), jnp.float32),
            pltpu.VMEM((batch, 2, tp // 2, length, span), jnp.bfloat16),
            pltpu.VMEM((batch, tp // 2, length, span), jnp.bfloat16),
            pltpu.VMEM((batch, tp // 2, length, span), jnp.bfloat16),
            pltpu.VMEM((batch, tp // 2 - 1, length, span), jnp.bfloat16),
            pltpu.SemaphoreType.DMA((batch,)),
            pltpu.SemaphoreType.DMA((batch,)),
            pltpu.SemaphoreType.DMA((batch, tp // 2 - 1)),
            pltpu.SemaphoreType.DMA((batch, tp // 2 - 1)),
            pltpu.SemaphoreType.DMA((2, 2, n // 2)),
            pltpu.SemaphoreType.DMA((2, 2, n // 2)),
            pltpu.SemaphoreType.DMA((2, len(plan))),
            pltpu.SemaphoreType.DMA((2, len(plan))),
        ],
        compiler_params=pltpu.CompilerParams(collective_id=0, has_side_effects=True, vmem_limit_bytes=60 * 1024 * 1024),
        name="layer",
    )(
        inputs,
        norm_gain.reshape(1, model),
        key_values,
        rest,
        query_gain,
        key_gain,
    )


def solution(mesh):
    in_specs = (
        P(None, "sp", None),
        P(),
        P("sp", None, "tp", None),
        P("sp", None, "tp", None),
        P("sp", None, "tp", None),
        P(),
        P(),
        P("tp", None, "sp"),
    )
    out_specs = P(None, "sp", "tp")
    run = functools.partial(body, mesh.shape["sp"], mesh.shape["tp"])
    return jax.shard_map(run, mesh=mesh, in_specs=in_specs, out_specs=out_specs, check_vma=False)
```

profile of v0, /device:TPU:228, one launch (start us, length us, event | category | flops | bytes accessed | tf_op | source)
XLA Modules:
  0.0 276.6 jit_solution(18353744741985553723)
XLA Ops:
  0.0 0.0 copy-start
  0.0 0.7 copy.15
  0.7 0.1 reshape.15
  0.8 0.0 copy-done
  0.8 0.1 reshape.14
  0.9 0.0 copy-start.1
  0.9 0.6 pad_maximum_fusion.1.wb_ref
  1.5 0.1 copy-done.1
  1.6 0.1 reshape.16
  1.7 0.0 copy-start.2
  1.7 0.7 copy-done.2
  2.4 0.1 reshape.17
  2.5 0.6 copy.14
  3.1 271.8 %layer.1 = bf16[4,128,256]{2,1,0:T(8,128)(2,1)} custom-call(bf16[4,128,1024]{2,1,0:T(8,128)(2,1)} %x_ref.1, f32[1,1024]{1,0:T(1,128)} %bitcast.7, bf16[8,768]{1,0:T(8,128)(2,1)} %bitcast.5, bf16[8,512]{1,0:T(8,128)(2,1)} %pad_maximum_fusion.1.wb_ref, f32[3,64]{1,0:T(4,128)} %qg_ref.1, f32[3,64]{1,0:T(4,128)} %kg_ref.1), custom_call_target="tpu_custom_call" | custom-call | tf_op jit(solution)/shard_map/layer/pallas_call | solution.py:339
  274.9 1.7 copy.19
  (3 shorter events, 0.0 us)
Async XLA Ops:
  0.0 0.8 copy-start
  0.9 0.7 copy-start.1
  1.7 0.7 copy-start.2
where the time goes:
time: 277 us
  Pallas kernels  272 us (98%)
  local copies, waits for them, and re-layouts  4.16 us (2%)
    pallas_call x1, Pallas kernels, body(): pl.pallas_call(functools.partial(layer_kernel, n, tp, batch, length, head...  272 us

commit v1 on v0

v1 whole, which is shorter than its diff:
```python
import functools
import math

import jax
import jax.numpy as jnp
from jax import lax
from jax.experimental import pallas as pl
from jax.experimental.pallas import tpu as pltpu
from jax.sharding import PartitionSpec as P

GAPS = ((1, 32), (4, 32), (16, 16))
REACH = tuple(d * h for d, h in GAPS)
EPS = 1e-06
NEG = -1e30
LOG2E = 1.4426950408889634
MESH = pl.DeviceIdType.MESH
NZ, NX = 16, 4
CHIPS = NZ * NX
WA, WB = 384, 256


def layer_kernel(
    tp, batch, length, x_ref, gain_ref, slab_ref, qg_ref, kg_ref, out_ref,
    wa, wb, wk, wq, nb, win0, win1, win2, qn, bias, osum, oown, orecv, wo, mown, msend, mrecv, mg,
    pair_send, pair_recv, local_sem, z_send, z_recv, x_send, x_recv, nb_send, nb_recv, halo_send, halo_recv,
    o_send, o_recv, oy_send, oy_recv, m_send, m_recv, y_send, y_recv,
):
    me = lax.axis_index("sp")
    mine = lax.axis_index("tp")
    groups = len(GAPS)
    core = me % 2
    other = 1 - core
    chip = me // 2
    x = chip % NX
    z = chip // NX
    rows = 2 * length
    wins = (win0, win1, win2)
    bufs = (wa, wb)

    def at_z(offset):
        return {"sp": (((z + offset + NZ) % NZ) * NX + x) * 2 + core}

    def at_x(offset):
        return {"sp": (z * NX + (x + offset) % NX) * 2 + core}

    sibling = {"sp": chip * 2 + other}

    def at_chip(offset):
        return {"sp": ((chip + offset + CHIPS) % CHIPS) * 2 + core}

    def at_y(offset):
        return {"tp": (mine + offset) % tp}

    barrier = pltpu.get_barrier_semaphore()

    def greet(target):
        pl.semaphore_signal(barrier, inc=1, device_id=target, device_id_type=MESH)

    targets = [at_z(o) for o in (-3, 3, -2, 2, -1, 1)] + [at_y(o) for o in range(1, tp)]
    targets += [at_x(o) for o in range(1, NX)] + [at_chip(1), at_chip(-1), sibling]
    for target in targets:
        greet(target)
    pl.semaphore_wait(barrier, len(targets))

    cuts = (pl.ds(0, WA), pl.ds(WA, WB))

    def pair(chunk):
        return pltpu.make_async_remote_copy(
            src_ref=slab_ref.at[other, :, cuts[chunk]],
            dst_ref=bufs[chunk].at[chip, core],
            send_sem=pair_send.at[chunk],
            recv_sem=pair_recv.at[chunk],
            device_id=sibling,
            device_id_type=MESH,
        )

    def local(chunk):
        return pltpu.make_async_copy(
            slab_ref.at[core, :, cuts[chunk]], bufs[chunk].at[chip, core], local_sem.at[chunk]
        )

    def z_copy(chunk, origin, step):
        index = ((z + origin + NZ) % NZ) * NX + x
        rel = (origin - step) % NZ
        block = bufs[chunk].at[index]
        return pltpu.make_async_remote_copy(
            src_ref=block,
            dst_ref=block,
            send_sem=z_send.at[chunk, rel],
            recv_sem=z_recv.at[chunk, rel],
            device_id=at_z(step),
            device_id_type=MESH,
        )

    def z_wait(chunk, origin):
        index = ((z + origin + NZ) % NZ) * NX + x
        block = bufs[chunk].at[index]
        pltpu.make_async_remote_copy(
            src_ref=block,
            dst_ref=block,
            send_sem=z_send.at[chunk, origin % NZ],
            recv_sem=z_recv.at[chunk, origin % NZ],
            device_id=at_z(1),
            device_id_type=MESH,
        ).wait_recv()

    sends = []

    def z_start(chunk, origin, step):
        copy = z_copy(chunk, origin, step)
        copy.start()
        sends.append(copy)

    def x_copy(chunk, origin, shift):
        block = bufs[chunk].at[((z + origin + NZ) % NZ) * NX + x]
        return pltpu.make_async_remote_copy(
            src_ref=block,
            dst_ref=block,
            send_sem=x_send.at[chunk, origin % NZ, shift - 1],
            recv_sem=x_recv.at[chunk, origin % NZ, shift - 1],
            device_id=at_x(shift),
            device_id_type=MESH,
        )

    def x_start(chunk, origin):
        for shift in (1, 3, 2):
            copy = x_copy(chunk, origin, shift)
            copy.start()
            sends.append(copy)

    def x_wait(chunk, origin, shift):
        block = bufs[chunk].at[((z + origin + NZ) % NZ) * NX + (x + NX - shift) % NX]
        pltpu.make_async_remote_copy(
            src_ref=block,
            dst_ref=block,
            send_sem=x_send.at[chunk, origin % NZ, shift - 1],
            recv_sem=x_recv.at[chunk, origin % NZ, shift - 1],
            device_id=at_x(1),
            device_id_type=MESH,
        ).wait_recv()

    for chunk in range(2):
        local(chunk).start()
        pair(chunk).start()
    for chunk in range(2):
        local(chunk).wait()
        pair(chunk).wait_recv()
        for step in (3, -3, 2, -2, 1, -1):
            z_start(chunk, 0, step)
    x_start(0, 0)

    def nb_copy(b):
        return pltpu.make_async_remote_copy(
            src_ref=nb.at[b, core],
            dst_ref=nb.at[b, core],
            send_sem=nb_send.at[b],
            recv_sem=nb_recv.at[b],
            device_id=sibling,
            device_id_type=MESH,
        )

    def norm_step(b, carry):
        flat = x_ref[b].astype(jnp.float32)
        scale = lax.rsqrt(jnp.mean(flat * flat, axis=-1, keepdims=True) + EPS)
        nb[b, core] = (flat * scale * gain_ref[...]).astype(jnp.bfloat16)
        nb_copy(b).start()
        return carry

    lax.fori_loop(0, batch, norm_step, 0)

    def relay(chunk, origin, spread):
        z_wait(chunk, origin)
        if origin in (3, 6):
            for step in (-3, -2, -1) if origin == 3 else (-1,) + ((-2,) if chunk == 1 else ()):
                z_start(chunk, origin, step)
        if origin in (-3, -6):
            for step in (3, 2, 1) if origin == -3 else (1,) + ((2,) if chunk == 0 else ()):
                z_start(chunk, origin, step)
        if spread:
            x_start(chunk, origin)

    for origin in (1, -1, 2, -2):
        relay(0, origin, True)
    for chunk in range(2):
        for origin in (3, -3):
            relay(chunk, origin, chunk == 0)

    head = mine * 2 + core
    heads = 2 * tp
    power = -8.0 * (head + 1).astype(jnp.float32) / heads
    slope = jnp.exp2(jnp.full((8, 128), power, jnp.float32))[:1, :1] * LOG2E
    widths = [length + 2 * r for r in REACH]
    starts = [sum(widths[:g]) for g in range(groups)]
    total_rows = CHIPS * rows

    def bias_step(block, carry):
        for group, (dilation, half) in enumerate(GAPS):
            reach = REACH[group]
            shape = (length, widths[group])
            key = lax.broadcasted_iota(jnp.int32, shape, 1) - reach
            offset = jnp.abs(key - lax.broadcasted_iota(jnp.int32, shape, 0))
            at = key + (chip * rows + block * length)
            allowed = (offset <= reach) & (at >= 0) & (at < total_rows) & ((offset & (dilation - 1)) == 0)
            value = jnp.where(allowed, offset.astype(jnp.float32) * (-slope / float(reach)), NEG)
            bias[block, :, starts[group] : starts[group] + widths[group]] = value
        return carry

    lax.fori_loop(0, 2, bias_step, 0)

    for origin in (4, -4, 5, -5):
        relay(0, origin, True)
    for chunk in range(2):
        for origin in (6, -6):
            relay(chunk, origin, chunk == 0)
    for origin in (7, -7, 8):
        relay(0, origin, True)
    x_start(1, 0)
    for origin in (3, -3, 6, -6):
        x_start(1, origin)
    for origin in (1, -1, 2, -2, 4, -4, 5, -5, 7, -7, 8):
        relay(1, origin, True)

    lane = lax.broadcasted_iota(jnp.int32, (rows, 128), 1)
    low = lane < 64

    def all_origins(chunk):
        for origin in (0, 1, -1, 2, -2, 3, -3, 4, -4, 5, -5, 6, -6, 7, -7, 8):
            for shift in (1, 3, 2):
                x_wait(chunk, origin, shift)

    all_origins(0)
    wk[...] = wa[...].reshape(2 * CHIPS * 8, WA)
    for b in range(batch):
        nb_copy(b).wait_recv()

    def halo(b, group, up):
        reach = REACH[group]
        win = wins[group]
        if up:
            src = win.at[b, pl.ds(rows, reach), :]
            dst = win.at[b, pl.ds(0, reach), :]
        else:
            src = win.at[b, pl.ds(reach, reach), :]
            dst = win.at[b, pl.ds(reach + rows, reach), :]
        return pltpu.make_async_remote_copy(
            src_ref=src,
            dst_ref=dst,
            send_sem=halo_send.at[b, group, 0 if up else 1],
            recv_sem=halo_recv.at[b, group, 0 if up else 1],
            device_id=at_chip(1 if up else -1),
            device_id_type=MESH,
        )

    def each_halo(b):
        return [halo(b, group, up) for group in (2, 1, 0) for up in (True, False)]

    ones = jnp.ones((1, 64), jnp.float32)
    zeros = jnp.zeros((1, 64), jnp.float32)

    def kv_step(b, carry):
        out = jnp.dot(nb[b].reshape(rows, -1), wk[...], preferred_element_type=jnp.float32)
        out = out.astype(jnp.bfloat16).astype(jnp.float32)
        for group in range(groups):
            seg = out[:, 128 * group : 128 * (group + 1)]
            mean = jnp.sum(jnp.where(low, seg * seg, 0.0), axis=-1, keepdims=True) / 64.0
            gain = jnp.concatenate([kg_ref[group : group + 1, :], ones], axis=1)
            scaled = seg * jnp.where(low, lax.rsqrt(mean + EPS), 1.0) * gain
            wins[group][b, REACH[group] : REACH[group] + rows, :] = scaled.astype(jnp.bfloat16)
        for copy in each_halo(b):
            copy.start()
        return carry

    lax.fori_loop(0, batch, kv_step, 0)

    all_origins(1)
    wq[...] = wb[...].reshape(2 * CHIPS * 8, WB)

    tile = wq[:, 128:].astype(jnp.float32)
    high = lax.broadcasted_iota(jnp.int32, tile.shape, 1) >= 64
    tile = jnp.where(high, tile, 0.0)
    tile = jnp.where(core == 0, pltpu.roll(tile, 64, 1), tile)
    oown[...] = tile.astype(jnp.bfloat16)
    o_pair = pltpu.make_async_remote_copy(
        src_ref=oown,
        dst_ref=orecv,
        send_sem=o_send.at[0],
        recv_sem=o_recv.at[0],
        device_id=sibling,
        device_id_type=MESH,
    )
    o_pair.start()

    factor = LOG2E / 8.0

    def q_step(b, carry):
        out = jnp.dot(nb[b].reshape(rows, -1), wq[...], preferred_element_type=jnp.float32)
        out = out.astype(jnp.bfloat16).astype(jnp.float32)
        first, second = out[:, :128], out[:, 128:]
        for group, seg, here in ((0, first, low), (1, first, ~low), (2, second, low)):
            mean = jnp.sum(jnp.where(here, seg * seg, 0.0), axis=-1, keepdims=True) / 64.0
            gain = qg_ref[group : group + 1, :] * factor
            gain = jnp.concatenate([zeros, gain] if group == 1 else [gain, zeros], axis=1)
            scaled = jnp.where(here, seg * lax.rsqrt(mean + EPS) * gain, 0.0)
            if group == 1:
                scaled = pltpu.roll(scaled, 64, 1)
            qn[group, b] = scaled.astype(jnp.bfloat16)
        return carry

    lax.fori_loop(0, batch, q_step, 0)

    span = wo.shape[1]
    o_pair.wait_recv()
    osum[...] = (oown[...] + orecv[...]).reshape(osum.shape)
    wo[mine] = osum[mine]

    def o_copy(shift):
        target = (mine + shift) % tp
        return pltpu.make_async_remote_copy(
            src_ref=osum.at[target],
            dst_ref=wo.at[mine],
            send_sem=oy_send.at[shift - 1],
            recv_sem=oy_recv.at[shift - 1],
            device_id=at_y(shift),
            device_id_type=MESH,
        )

    def o_wait(shift):
        pltpu.make_async_remote_copy(
            src_ref=osum.at[mine],
            dst_ref=wo.at[(mine + tp - shift) % tp],
            send_sem=oy_send.at[shift - 1],
            recv_sem=oy_recv.at[shift - 1],
            device_id=at_y(shift),
            device_id_type=MESH,
        ).wait_recv()

    for shift in range(1, tp):
        o_copy(shift).start()

    keep = lax.broadcasted_iota(jnp.int32, (length, 128), 1) >= 64

    def attend(b, block):
        total = jnp.zeros((length, 1), jnp.float32)
        summed = jnp.zeros((length, 128), jnp.float32)
        begin = pl.multiple_of(block * length, length)
        for group in range(groups):
            query = qn[group, b, pl.ds(begin, length), :]
            window = wins[group][b, pl.ds(begin, widths[group]), :]
            scores = lax.dot_general(query, window, (((1,), (1,)), ((), ())), preferred_element_type=jnp.float32)
            grown = jnp.exp2(scores + bias[block, :, starts[group] : starts[group] + widths[group]])
            total = total + jnp.sum(grown, axis=-1, keepdims=True)
            summed = summed + jnp.dot(grown.astype(jnp.bfloat16), window, preferred_element_type=jnp.float32)
        merged = jnp.where(keep, summed / total, 0.0)
        return jnp.where(core == 0, pltpu.roll(merged, 64, 1), merged).astype(jnp.bfloat16)

    def m_copy(b):
        return pltpu.make_async_remote_copy(
            src_ref=msend.at[b],
            dst_ref=mrecv.at[b],
            send_sem=m_send.at[b],
            recv_sem=m_recv.at[b],
            device_id=sibling,
            device_id_type=MESH,
        )

    def y_copy(b, shift):
        return pltpu.make_async_remote_copy(
            src_ref=mg.at[mine, b],
            dst_ref=mg.at[mine, b],
            send_sem=y_send.at[b, shift - 1],
            recv_sem=y_recv.at[b, shift - 1],
            device_id=at_y(shift),
            device_id_type=MESH,
        )

    def y_wait(b, shift):
        block = mg.at[(mine + tp - shift) % tp, b]
        pltpu.make_async_remote_copy(
            src_ref=block,
            dst_ref=block,
            send_sem=y_send.at[b, shift - 1],
            recv_sem=y_recv.at[b, shift - 1],
            device_id=at_y(shift),
            device_id_type=MESH,
        ).wait_recv()

    def pass_on(b):
        m_copy(b).wait_recv()
        mg[mine, b] = mown[b] + mrecv[b]
        for shift in range(1, tp):
            y_copy(b, shift).start()

    def attend_step(b, carry):
        for copy in each_halo(b):
            copy.wait_recv()
        msend[b] = attend(b, other)
        m_copy(b).start()

        @pl.when(b >= 1)
        def _():
            pass_on(b - 1)

        mown[b] = attend(b, core)
        return carry

    lax.fori_loop(0, batch, attend_step, 0)
    pass_on(batch - 1)
    for shift in range(1, tp):
        o_wait(shift)

    def finish(b, carry):
        for shift in range(1, tp):
            y_wait(b, shift)
        final = jnp.zeros((length, span), jnp.float32)
        for part in range(tp):
            final = final + lax.dot_general(
                mg[part, b], wo[part], (((1,), (1,)), ((), ())), preferred_element_type=jnp.float32
            )
        out_ref[b] = final.astype(jnp.bfloat16)
        for shift in range(1, tp):
            y_copy(b, shift).wait_send()
        m_copy(b).wait_send()
        nb_copy(b).wait_send()
        for copy in each_halo(b):
            copy.wait_send()
        return carry

    lax.fori_loop(0, batch, finish, 0)
    for copy in sends:
        copy.wait_send()
    for chunk in range(2):
        pair(chunk).wait_send()
    o_pair.wait_send()
    for shift in range(1, tp):
        o_copy(shift).wait_send()


def body(tp, inputs, norm_gain, query_weight, key_weight, value_weight, query_gain, key_gain, out_weight):
    batch, length, model = inputs.shape
    share, groups, heads, width = query_weight.shape
    pairs = jnp.stack([key_weight, value_weight], axis=3).transpose(2, 0, 1, 3, 4).reshape(heads, share, WA)
    queries = query_weight.transpose(2, 0, 1, 3).reshape(heads, share, groups * width)
    slab = jnp.concatenate([pairs, queries, out_weight.transpose(0, 2, 1)], axis=2)
    span = model // tp
    rows = 2 * length
    total = sum(length + 2 * r for r in REACH)
    vmem = pl.BlockSpec(memory_space=pltpu.VMEM)
    bf16 = jnp.bfloat16
    dma = pltpu.SemaphoreType.DMA
    return pl.pallas_call(
        functools.partial(layer_kernel, tp, batch, length),
        out_shape=jax.ShapeDtypeStruct((batch, length, span), bf16),
        in_specs=[vmem] * 5,
        out_specs=vmem,
        scratch_shapes=[
            pltpu.VMEM((CHIPS, 2, share, WA), bf16),
            pltpu.VMEM((CHIPS, 2, share, WB), bf16),
            pltpu.VMEM((model, WA), bf16),
            pltpu.VMEM((model, WB), bf16),
            pltpu.VMEM((batch, 2, length, model), bf16),
            *[pltpu.VMEM((batch, rows + 2 * r, 128), bf16) for r in REACH],
            pltpu.VMEM((groups, batch, rows, 128), bf16),
            pltpu.VMEM((2, length, total), jnp.float32),
            pltpu.VMEM((tp, span, 128), bf16),
            pltpu.VMEM((model, 128), bf16),
            pltpu.VMEM((model, 128), bf16),
            pltpu.VMEM((tp, span, 128), bf16),
            pltpu.VMEM((batch, length, 128), bf16),
            pltpu.VMEM((batch, length, 128), bf16),
            pltpu.VMEM((batch, length, 128), bf16),
            pltpu.VMEM((tp, batch, length, 128), bf16),
            dma((2,)),
            dma((2,)),
            dma((2,)),
            dma((2, NZ)),
            dma((2, NZ)),
            dma((2, NZ, 3)),
            dma((2, NZ, 3)),
            dma((batch,)),
            dma((batch,)),
            dma((batch, groups, 2)),
            dma((batch, groups, 2)),
            dma((1,)),
            dma((1,)),
            dma((tp - 1,)),
            dma((tp - 1,)),
            dma((batch,)),
            dma((batch,)),
            dma((batch, tp - 1)),
            dma((batch, tp - 1)),
        ],
        compiler_params=pltpu.CompilerParams(collective_id=0, has_side_effects=True, vmem_limit_bytes=60 * 1024 * 1024),
        name="layer",
    )(
        inputs,
        norm_gain.reshape(1, model),
        slab,
        query_gain,
        key_gain,
    )


def solution(mesh):
    in_specs = (
        P(None, "sp", None),
        P(),
        P("sp", None, "tp", None),
        P("sp", None, "tp", None),
        P("sp", None, "tp", None),
        P(),
        P(),
        P("tp", None, "sp"),
    )
    out_specs = P(None, "sp", "tp")
    run = functools.partial(body, mesh.shape["tp"])
    return jax.shard_map(run, mesh=mesh, in_specs=in_specs, out_specs=out_specs, check_vma=False)
```

time: 277 us -> 68.8 us (0.25)
  the two profiles are of different devices: /device:TPU:228 before, /device:TPU:1 now
where the time goes in v1:
time: 68.8 us; the launch traced here: 68.5 us
  Pallas kernels  63.9 us (93%)
  local copies, waits for them, and re-layouts  3.8 us (6%)
  other arithmetic  0.73 us (1%)
    pallas_call x1, Pallas kernels, body(): pl.pallas_call(functools.partial(layer_kernel, tp, batch, length), out_sh...  63.9 us
    unnamed x7, local copies, waits for them, and re-layouts  2.88 us

profile of v1, /device:TPU:1, one launch (start us, length us, event | category | flops | bytes accessed | tf_op | source)
XLA Modules:
  0.0 68.5 jit_solution(17664064573726334797)
XLA Ops:
  0.0 0.7 %copy.12 = bf16[2,8,3,64]{3,2,1,0:T(4,128)(2,1)S(1)} copy(bf16[2,8,3,64]{3,0,2,1:T(2,128)(2,1)} %bitcast.7) | data formatting | bytes 12288 | tf_op jit(solution)/shard_map/transpose | solution.py:442
  0.7 0.0 copy-start
  0.7 0.0 copy-start.1
  0.7 0.1 reshape.11
  0.8 0.6 copy-done
  1.4 0.0 copy-done.1
  1.5 0.0 copy-start.2
  1.5 0.1 reshape.10
  1.6 0.6 copy-done.2
  2.2 0.7 pad_maximum_fusion.slab_ref
  2.9 63.9 %layer.1 = bf16[4,128,256]{2,1,0:T(8,128)(2,1)} custom-call(bf16[4,128,1024]{2,1,0:T(8,128)(2,1)} %x_ref.1, f32[1,1024]{1,0:T(1,128)} %bitcast.10, bf16[2,8,640]{2,1,0:T(8,128)(2,1)} %pad_maximum_fusion.slab_ref, f32[3,64]{1,0:T(4,128)} %qg_ref.1, f32[3,64]{1,0:T(4,128)} %kg_ref.1), custom_call_target="tpu_custom_call" | custom-call | tf_op jit(solution)/shard_map/layer/pallas_call | solution.py:450
  66.8 1.7 %copy.14 = bf16[4,128,256]{2,1,0:T(8,128)(2,1)} copy(bf16[4,128,256]{2,1,0:T(8,128)(2,1)} %layer.1) | data formatting | bytes 524288
  (2 shorter events, 0.1 us)
Async XLA Ops:
  0.7 0.7 %copy-start = (bf16[8,3,2,64]{3,2,1,0:T(2,128)(2,1)S(1)}, bf16[8,3,2,64]{3,2,1,0:T(2,128)(2,1)}, u32[]{:S(2)}) copy-start(bf16[8,3,2,64]{3,2,1,0:T(2,128)(2,1)} %param.12) | copy-start | bytes 18436
  0.7 0.7 %copy-start.1 = (bf16[8,3,2,64]{3,2,1,0:T(2,128)(2,1)S(1)}, bf16[8,3,2,64]{3,2,1,0:T(2,128)(2,1)}, u32[]{:S(2)}) copy-start(bf16[8,3,2,64]{3,2,1,0:T(2,128)(2,1)} %param.11) | copy-start | bytes 18436
  1.5 0.7 %copy-start.2 = (bf16[2,64,8]{1,2,0:T(8,128)(2,1)S(1)}, bf16[2,64,8]{1,2,0:T(8,128)(2,1)}, u32[]{:S(2)}) copy-start(bf16[2,64,8]{1,2,0:T(8,128)(2,1)} %param.15) | copy-start | bytes 6148

commit v2 on v1

--- a/solution.py
+++ b/solution.py
@@ -16,13 +16,15 @@
 MESH = pl.DeviceIdType.MESH
 NZ, NX = 16, 4
 CHIPS = NZ * NX
-WA, WB = 384, 256
+WB = 256
 
 
 def layer_kernel(
-    tp, batch, length, x_ref, gain_ref, slab_ref, qg_ref, kg_ref, out_ref,
-    wa, wb, wk, wq, nb, win0, win1, win2, qn, bias, osum, oown, orecv, wo, mown, msend, mrecv, mg,
-    pair_send, pair_recv, local_sem, z_send, z_recv, x_send, x_recv, nb_send, nb_recv, halo_send, halo_recv,
+    tp, batch, length, x_hbm, gain_hbm, qw_hbm, kw_hbm, vw_hbm, ow_hbm, qg_hbm, kg_hbm, out_ref,
+    x_ref, gain_ref, qw_ref, kw_ref, vw_ref, ow_ref, qg_ref, kg_ref, slab_ref,
+    w2, w01, wb, wk2, wk01, wq, nb, win0, win1, win2, qn, bias, osum, oown, orecv, wo, mown, msend, mrecv, mg,
+    in_sem, pair_send, pair_recv, local_sem, za_send, za_recv, xa_send, xa_recv, zb_send, zb_recv, xb_send, xb_recv,
+    nb_send, nb_recv, halo_send, halo_recv,
     o_send, o_recv, oy_send, oy_recv, m_send, m_recv, y_send, y_recv,
 ):
     me = lax.axis_index("sp")
@@ -35,7 +37,7 @@
     z = chip // NX
     rows = 2 * length
     wins = (win0, win1, win2)
-    bufs = (wa, wb)
+    bufs = (w2, w01, wb)
 
     def at_z(offset):
         return {"sp": (((z + offset + NZ) % NZ) * NX + x) * 2 + core}
@@ -56,13 +58,41 @@
     def greet(target):
         pl.semaphore_signal(barrier, inc=1, device_id=target, device_id_type=MESH)
 
-    targets = [at_z(o) for o in (-3, 3, -2, 2, -1, 1)] + [at_y(o) for o in range(1, tp)]
+    targets = [at_z(o) for o in (-4, 4, -3, 3, -2, 2, -1, 1)] + [at_y(o) for o in range(1, tp)]
     targets += [at_x(o) for o in range(1, NX)] + [at_chip(1), at_chip(-1), sibling]
     for target in targets:
         greet(target)
+
+    fetches = [
+        pltpu.make_async_copy(src, dst, in_sem.at[i])
+        for i, (src, dst) in enumerate(
+            (
+                (qw_hbm, qw_ref),
+                (kw_hbm, kw_ref),
+                (vw_hbm, vw_ref),
+                (ow_hbm, ow_ref),
+                (qg_hbm, qg_ref),
+                (kg_hbm, kg_ref),
+                (gain_hbm, gain_ref),
+                (x_hbm, x_ref),
+            )
+        )
+    ]
+    for fetch in fetches:
+        fetch.start()
+    for fetch in fetches[:4]:
+        fetch.wait()
+    for head in range(2):
+        pieces = []
+        for group in (2, 0, 1):
+            pieces += [kw_ref[:, group, head, :], vw_ref[:, group, head, :]]
+        pieces += [qw_ref[:, group, head, :] for group in range(groups)]
+        pieces = [piece.astype(jnp.float32) for piece in pieces + [ow_ref[head]]]
+        slab_ref[head] = jnp.concatenate(pieces, axis=1).astype(jnp.bfloat16)
+
     pl.semaphore_wait(barrier, len(targets))
 
-    cuts = (pl.ds(0, WA), pl.ds(WA, WB))
+    cuts = (pl.ds(0, 128), pl.ds(128, 256), pl.ds(384, WB))
 
     def pair(chunk):
         return pltpu.make_async_remote_copy(
@@ -79,75 +109,78 @@
             slab_ref.at[core, :, cuts[chunk]], bufs[chunk].at[chip, core], local_sem.at[chunk]
         )
 
-    def z_copy(chunk, origin, step):
-        index = ((z + origin + NZ) % NZ) * NX + x
-        rel = (origin - step) % NZ
-        block = bufs[chunk].at[index]
-        return pltpu.make_async_remote_copy(
-            src_ref=block,
-            dst_ref=block,
-            send_sem=z_send.at[chunk, rel],
-            recv_sem=z_recv.at[chunk, rel],
-            device_id=at_z(step),
-            device_id_type=MESH,
-        )
-
-    def z_wait(chunk, origin):
-        index = ((z + origin + NZ) % NZ) * NX + x
-        block = bufs[chunk].at[index]
-        pltpu.make_async_remote_copy(
-            src_ref=block,
-            dst_ref=block,
-            send_sem=z_send.at[chunk, origin % NZ],
-            recv_sem=z_recv.at[chunk, origin % NZ],
-            device_id=at_z(1),
-            device_id_type=MESH,
-        ).wait_recv()
+    def index_of(origin, column):
+        return ((z + origin + NZ) % NZ) * NX + (x + column) % NX
 
     sends = []
 
-    def z_start(chunk, origin, step):
-        copy = z_copy(chunk, origin, step)
+    def move(block, send_sem, recv_sem, target):
+        return pltpu.make_async_remote_copy(
+            src_ref=block, dst_ref=block, send_sem=send_sem, recv_sem=recv_sem, device_id=target, device_id_type=MESH
+        )
+
+    def begin(copy):
         copy.start()
         sends.append(copy)
 
-    def x_copy(chunk, origin, shift):
-        block = bufs[chunk].at[((z + origin + NZ) % NZ) * NX + x]
-        return pltpu.make_async_remote_copy(
-            src_ref=block,
-            dst_ref=block,
-            send_sem=x_send.at[chunk, origin % NZ, shift - 1],
-            recv_sem=x_recv.at[chunk, origin % NZ, shift - 1],
-            device_id=at_x(shift),
-            device_id_type=MESH,
-        )
-
-    def x_start(chunk, origin):
+    def za_start(chunk, origin, step):
+        rel = (origin - step) % NZ
+        block = bufs[chunk].at[index_of(origin, 0)]
+        begin(move(block, za_send.at[chunk, rel], za_recv.at[chunk, rel], at_z(step)))
+
+    def za_wait(chunk, origin):
+        rel = origin % NZ
+        block = bufs[chunk].at[index_of(origin, 0)]
+        move(block, za_send.at[chunk, rel], za_recv.at[chunk, rel], at_z(1)).wait_recv()
+
+    def xa_start(chunk, origin):
+        rel = origin % NZ
+        block = bufs[chunk].at[index_of(origin, 0)]
         for shift in (1, 3, 2):
-            copy = x_copy(chunk, origin, shift)
-            copy.start()
-            sends.append(copy)
-
-    def x_wait(chunk, origin, shift):
-        block = bufs[chunk].at[((z + origin + NZ) % NZ) * NX + (x + NX - shift) % NX]
-        pltpu.make_async_remote_copy(
-            src_ref=block,
-            dst_ref=block,
-            send_sem=x_send.at[chunk, origin % NZ, shift - 1],
-            recv_sem=x_recv.at[chunk, origin % NZ, shift - 1],
-            device_id=at_x(1),
-            device_id_type=MESH,
-        ).wait_recv()
-
-    for chunk in range(2):
+            begin(move(block, xa_send.at[chunk, rel, shift - 1], xa_recv.at[chunk, rel, shift - 1], at_x(shift)))
+
+    def xa_wait(chunk, origin, shift):
+        rel = origin % NZ
+        block = bufs[chunk].at[index_of(origin, NX - shift)]
+        move(block, xa_send.at[chunk, rel, shift - 1], xa_recv.at[chunk, rel, shift - 1], at_x(1)).wait_recv()
+
+    def xb_start():
+        block = wb.at[chip]
+        for shift in (1, 3, 2):
+            begin(move(block, xb_send.at[shift - 1], xb_recv.at[shift - 1], at_x(shift)))
+
+    def xb_wait(shift):
+        block = wb.at[index_of(0, NX - shift)]
+        move(block, xb_send.at[shift - 1], xb_recv.at[shift - 1], at_x(1)).wait_recv()
+
+    def zb_start(origin, step, column):
+        rel = (origin - step) % NZ
+        block = wb.at[index_of(origin, column)]
+        begin(move(block, zb_send.at[rel, column], zb_recv.at[rel, column], at_z(step)))
+
+    def zb_wait(origin, column):
+        rel = origin % NZ
+        block = wb.at[index_of(origin, column)]
+        move(block, zb_send.at[rel, column], zb_recv.at[rel, column], at_z(1)).wait_recv()
+
+    far = {4: ((-3, -1, -2), (-4, -3, -1, -2)), -4: ((4, 3, 1, 2), (3, 1, 2))}
+    spread = (4, -4, 1, -1, 2, -2, 3, -3)
+
+    for chunk in range(3):
         local(chunk).start()
         pair(chunk).start()
     for chunk in range(2):
         local(chunk).wait()
         pair(chunk).wait_recv()
-        for step in (3, -3, 2, -2, 1, -1):
-            z_start(chunk, 0, step)
-    x_start(0, 0)
+        for step in spread:
+            za_start(chunk, 0, step)
+    local(2).wait()
+    pair(2).wait_recv()
+    xb_start()
+    for chunk in range(2):
+        xa_start(chunk, 0)
+    for step in spread:
+        zb_start(0, step, 0)
 
     def nb_copy(b):
         return pltpu.make_async_remote_copy(
@@ -166,24 +199,28 @@
         nb_copy(b).start()
         return carry
 
+    for fetch in fetches[4:]:
+        fetch.wait()
     lax.fori_loop(0, batch, norm_step, 0)
 
-    def relay(chunk, origin, spread):
-        z_wait(chunk, origin)
-        if origin in (3, 6):
-            for step in (-3, -2, -1) if origin == 3 else (-1,) + ((-2,) if chunk == 1 else ()):
-                z_start(chunk, origin, step)
-        if origin in (-3, -6):
-            for step in (3, 2, 1) if origin == -3 else (1,) + ((2,) if chunk == 0 else ()):
-                z_start(chunk, origin, step)
-        if spread:
-            x_start(chunk, origin)
-
     for origin in (1, -1, 2, -2):
-        relay(0, origin, True)
-    for chunk in range(2):
-        for origin in (3, -3):
-            relay(chunk, origin, chunk == 0)
+        for chunk in range(2):
+            za_wait(chunk, origin)
+            xa_start(chunk, origin)
+    for origin in (4, -4):
+        for chunk in range(2):
+            za_wait(chunk, origin)
+            for step in far[origin][chunk]:
+                za_start(chunk, origin, step)
+            xa_start(chunk, origin)
+    for origin in (3, -3):
+        for chunk in range(2):
+            za_wait(chunk, origin)
+            xa_start(chunk, origin)
+    for shift in (1, 3, 2):
+        xb_wait(shift)
+        for step in spread:
+            zb_start(0, step, NX - shift)
 
     head = mine * 2 + core
     heads = 2 * tp
@@ -207,29 +244,34 @@
 
     lax.fori_loop(0, 2, bias_step, 0)
 
-    for origin in (4, -4, 5, -5):
-        relay(0, origin, True)
-    for chunk in range(2):
-        for origin in (6, -6):
-            relay(chunk, origin, chunk == 0)
-    for origin in (7, -7, 8):
-        relay(0, origin, True)
-    x_start(1, 0)
-    for origin in (3, -3, 6, -6):
-        x_start(1, origin)
-    for origin in (1, -1, 2, -2, 4, -4, 5, -5, 7, -7, 8):
-        relay(1, origin, True)
+    late = (5, -5, 6, -6, 7, -7, 8)
+    for origin in (4, -4):
+        zb_wait(origin, 0)
+        for step in far[origin][0]:
+            zb_start(origin, step, 0)
+    for origin in late:
+        za_wait(0, origin)
+        xa_start(0, origin)
+    for column in (3, 1, 2):
+        for origin in (4, -4):
+            zb_wait(origin, column)
+            for step in far[origin][column % 2]:
+                zb_start(origin, step, column)
+    for origin in late:
+        za_wait(1, origin)
+        xa_start(1, origin)
 
     lane = lax.broadcasted_iota(jnp.int32, (rows, 128), 1)
     low = lane < 64
-
-    def all_origins(chunk):
-        for origin in (0, 1, -1, 2, -2, 3, -3, 4, -4, 5, -5, 6, -6, 7, -7, 8):
+    origins = (0, 1, -1, 2, -2, 3, -3, 4, -4) + late
+
+    def all_keys(chunk):
+        for origin in origins:
             for shift in (1, 3, 2):
-                x_wait(chunk, origin, shift)
-
-    all_origins(0)
-    wk[...] = wa[...].reshape(2 * CHIPS * 8, WA)
+                xa_wait(chunk, origin, shift)
+
+    all_keys(0)
+    wk2[...] = w2[...].reshape(wk2.shape)
     for b in range(batch):
         nb_copy(b).wait_recv()
 
@@ -251,29 +293,37 @@
             device_id_type=MESH,
         )
 
-    def each_halo(b):
-        return [halo(b, group, up) for group in (2, 1, 0) for up in (True, False)]
+    def each_halo(b, only=(2, 1, 0)):
+        return [halo(b, group, up) for group in only for up in (True, False)]
 
     ones = jnp.ones((1, 64), jnp.float32)
     zeros = jnp.zeros((1, 64), jnp.float32)
 
-    def kv_step(b, carry):
-        out = jnp.dot(nb[b].reshape(rows, -1), wk[...], preferred_element_type=jnp.float32)
-        out = out.astype(jnp.bfloat16).astype(jnp.float32)
-        for group in range(groups):
-            seg = out[:, 128 * group : 128 * (group + 1)]
-            mean = jnp.sum(jnp.where(low, seg * seg, 0.0), axis=-1, keepdims=True) / 64.0
-            gain = jnp.concatenate([kg_ref[group : group + 1, :], ones], axis=1)
-            scaled = seg * jnp.where(low, lax.rsqrt(mean + EPS), 1.0) * gain
-            wins[group][b, REACH[group] : REACH[group] + rows, :] = scaled.astype(jnp.bfloat16)
-        for copy in each_halo(b):
-            copy.start()
-        return carry
-
-    lax.fori_loop(0, batch, kv_step, 0)
-
-    all_origins(1)
-    wq[...] = wb[...].reshape(2 * CHIPS * 8, WB)
+    def kv_step(weights, order):
+        def step(b, carry):
+            out = jnp.dot(nb[b].reshape(rows, -1), weights[...], preferred_element_type=jnp.float32)
+            out = out.astype(jnp.bfloat16).astype(jnp.float32)
+            for place, group in enumerate(order):
+                seg = out[:, 128 * place : 128 * (place + 1)]
+                mean = jnp.sum(jnp.where(low, seg * seg, 0.0), axis=-1, keepdims=True) / 64.0
+                gain = jnp.concatenate([kg_ref[group : group + 1, :], ones], axis=1)
+                scaled = seg * jnp.where(low, lax.rsqrt(mean + EPS), 1.0) * gain
+                wins[group][b, REACH[group] : REACH[group] + rows, :] = scaled.astype(jnp.bfloat16)
+            for copy in each_halo(b, order):
+                copy.start()
+            return carry
+
+        return step
+
+    lax.fori_loop(0, batch, kv_step(wk2, (2,)), 0)
+    all_keys(1)
+    wk01[...] = w01[...].reshape(wk01.shape)
+    lax.fori_loop(0, batch, kv_step(wk01, (0, 1)), 0)
+
+    for origin in (1, -1, 2, -2, 3, -3) + late:
+        for column in range(NX):
+            zb_wait(origin, column)
+    wq[...] = wb[...].reshape(wq.shape)
 
     tile = wq[:, 128:].astype(jnp.float32)
     high = lax.broadcasted_iota(jnp.int32, tile.shape, 1) >= 64
@@ -428,7 +478,7 @@
     lax.fori_loop(0, batch, finish, 0)
     for copy in sends:
         copy.wait_send()
-    for chunk in range(2):
+    for chunk in range(3):
         pair(chunk).wait_send()
     o_pair.wait_send()
     for shift in range(1, tp):
@@ -438,24 +488,34 @@
 def body(tp, inputs, norm_gain, query_weight, key_weight, value_weight, query_gain, key_gain, out_weight):
     batch, length, model = inputs.shape
     share, groups, heads, width = query_weight.shape
-    pairs = jnp.stack([key_weight, value_weight], axis=3).transpose(2, 0, 1, 3, 4).reshape(heads, share, WA)
-    queries = query_weight.transpose(2, 0, 1, 3).reshape(heads, share, groups * width)
-    slab = jnp.concatenate([pairs, queries, out_weight.transpose(0, 2, 1)], axis=2)
     span = model // tp
     rows = 2 * length
     total = sum(length + 2 * r for r in REACH)
-    vmem = pl.BlockSpec(memory_space=pltpu.VMEM)
     bf16 = jnp.bfloat16
     dma = pltpu.SemaphoreType.DMA
+    operands = (
+        inputs,
+        norm_gain.reshape(1, model),
+        query_weight,
+        key_weight,
+        value_weight,
+        out_weight.transpose(0, 2, 1),
+        query_gain,
+        key_gain,
+    )
     return pl.pallas_call(
         functools.partial(layer_kernel, tp, batch, length),
         out_shape=jax.ShapeDtypeStruct((batch, length, span), bf16),
-        in_specs=[vmem] * 5,
-        out_specs=vmem,
+        in_specs=[pl.BlockSpec(memory_space=pl.ANY)] * len(operands),
+        out_specs=pl.BlockSpec(memory_space=pltpu.VMEM),
         scratch_shapes=[
-            pltpu.VMEM((CHIPS, 2, share, WA), bf16),
+            *[pltpu.VMEM(operand.shape, operand.dtype) for operand in operands],
+            pltpu.VMEM((heads, share, 384 + WB), bf16),
+            pltpu.VMEM((CHIPS, 2, share, 128), bf16),
+            pltpu.VMEM((CHIPS, 2, share, 256), bf16),
             pltpu.VMEM((CHIPS, 2, share, WB), bf16),
-            pltpu.VMEM((model, WA), bf16),
+            pltpu.VMEM((model, 128), bf16),
+            pltpu.VMEM((model, 256), bf16),
             pltpu.VMEM((model, WB), bf16),
             pltpu.VMEM((batch, 2, length, model), bf16),
             *[pltpu.VMEM((batch, rows + 2 * r, 128), bf16) for r in REACH],
@@ -469,13 +529,18 @@
             pltpu.VMEM((batch, length, 128), bf16),
             pltpu.VMEM((batch, length, 128), bf16),
             pltpu.VMEM((tp, batch, length, 128), bf16),
-            dma((2,)),
-            dma((2,)),
-            dma((2,)),
+            dma((len(operands),)),
+            dma((3,)),
+            dma((3,)),
+            dma((3,)),
             dma((2, NZ)),
             dma((2, NZ)),
             dma((2, NZ, 3)),
             dma((2, NZ, 3)),
+            dma((NZ, NX)),
+            dma((NZ, NX)),
+            dma((3,)),
+            dma((3,)),
             dma((batch,)),
             dma((batch,)),
             dma((batch, groups, 2)),
@@ -491,13 +556,7 @@
         ],
         compiler_params=pltpu.CompilerParams(collective_id=0, has_side_effects=True, vmem_limit_bytes=60 * 1024 * 1024),
         name="layer",
-    )(
-        inputs,
-        norm_gain.reshape(1, model),
-        slab,
-        query_gain,
-        key_gain,
-    )
+    )(*operands)
 
 
 def solution(mesh):

time: 68.8 us -> 63.9 us (0.929)
  the two profiles are of different devices: /device:TPU:1 before, /device:TPU:96 now
where the time goes in v2:
time: 63.9 us; the launch traced here: 63.7 us
  Pallas kernels  62 us (97%)
  local copies, waits for them, and re-layouts  1.67 us (3%)
    pallas_call x1, Pallas kernels, body(): pl.pallas_call(functools.partial(layer_kernel, tp, batch, length), out_sh...  62 us
    unnamed x1, local copies, waits for them, and re-layouts  1.67 us

profile of v2, /device:TPU:96, one launch (start us, length us, event | category | flops | bytes accessed | tf_op | source)
XLA Modules:
  0.0 63.7 jit_solution(4016462416730251326)
XLA Ops:
  0.0 62.0 %layer.1 = bf16[4,128,256]{2,1,0:T(8,128)(2,1)} custom-call(bf16[4,128,1024]{2,1,0:T(8,128)(2,1)} %x_hbm.1, f32[1,1024]{1,0:T(1,128)} %bitcast.2, bf16[8,3,2,64]{3,2,1,0:T(2,128)(2,1)} %qw_hbm.1, bf16[8,3,2,64]{3,2,1,0:T(2,128)(2,1)} %kw_hbm.1, bf16[8,3,2,64]{3,2,1,0:T(2,128)(2,1)} %vw_hbm.1, bf16[2,8,64]{2,1,0:T(8,128)(2,1)} %bitcast.3, f32[3,64]{1,0:T(4,128)} %qg_hbm.1, ...), custom_call_target="tpu_custom_call" | custom-call | tf_op jit(solution)/shard_map/layer/pallas_call | solution.py:506
  62.0 1.7 %copy.10 = bf16[4,128,256]{2,1,0:T(8,128)(2,1)} copy(bf16[4,128,256]{2,1,0:T(8,128)(2,1)} %layer.1) | data formatting | bytes 524288

commit v3 on v2

--- a/solution.py
+++ b/solution.py
@@ -23,7 +23,7 @@
     tp, batch, length, x_hbm, gain_hbm, qw_hbm, kw_hbm, vw_hbm, ow_hbm, qg_hbm, kg_hbm, out_ref,
     x_ref, gain_ref, qw_ref, kw_ref, vw_ref, ow_ref, qg_ref, kg_ref, slab_ref,
     w2, w01, wb, wk2, wk01, wq, nb, win0, win1, win2, qn, bias, osum, oown, orecv, wo, mown, msend, mrecv, mg,
-    in_sem, pair_send, pair_recv, local_sem, za_send, za_recv, xa_send, xa_recv, zb_send, zb_recv, xb_send, xb_recv,
+    in_sem, pair_send, pair_recv, local_sem, zh_send, zh_recv, za_send, za_recv, xa_send, xa_recv,
     nb_send, nb_recv, halo_send, halo_recv,
     o_send, o_recv, oy_send, oy_recv, m_send, m_recv, y_send, y_recv,
 ):
@@ -39,8 +39,8 @@
     wins = (win0, win1, win2)
     bufs = (w2, w01, wb)
 
-    def at_z(offset):
-        return {"sp": (((z + offset + NZ) % NZ) * NX + x) * 2 + core}
+    def at_z(offset, on=core):
+        return {"sp": (((z + offset + NZ) % NZ) * NX + x) * 2 + on}
 
     def at_x(offset):
         return {"sp": (z * NX + (x + offset) % NX) * 2 + core}
@@ -60,6 +60,7 @@
 
     targets = [at_z(o) for o in (-4, 4, -3, 3, -2, 2, -1, 1)] + [at_y(o) for o in range(1, tp)]
     targets += [at_x(o) for o in range(1, NX)] + [at_chip(1), at_chip(-1), sibling]
+    targets += [at_z(o, other) for o in (-4, 4, -3, 3, -2, 2, -1, 1)]
     for target in targets:
         greet(target)
 
@@ -123,6 +124,32 @@
         copy.start()
         sends.append(copy)
 
+    def zh_start(chunk, step):
+        rel = -step % NZ
+        for half, on in enumerate((core, other)):
+            begin(
+                pltpu.make_async_remote_copy(
+                    src_ref=slab_ref.at[on, :, cuts[chunk]],
+                    dst_ref=bufs[chunk].at[chip, core],
+                    send_sem=zh_send.at[chunk, rel, half],
+                    recv_sem=zh_recv.at[chunk, rel, half],
+                    device_id=at_z(step, on),
+                    device_id_type=MESH,
+                )
+            )
+
+    def zh_wait(chunk, origin):
+        rel = origin % NZ
+        for half, parity in enumerate((core, other)):
+            pltpu.make_async_remote_copy(
+                src_ref=slab_ref.at[0, :, cuts[chunk]],
+                dst_ref=bufs[chunk].at[index_of(origin, 0), parity],
+                send_sem=zh_send.at[chunk, rel, half],
+                recv_sem=zh_recv.at[chunk, rel, half],
+                device_id=at_z(1),
+                device_id_type=MESH,
+            ).wait_recv()
+
     def za_start(chunk, origin, step):
         rel = (origin - step) % NZ
         block = bufs[chunk].at[index_of(origin, 0)]
@@ -144,43 +171,13 @@
         block = bufs[chunk].at[index_of(origin, NX - shift)]
         move(block, xa_send.at[chunk, rel, shift - 1], xa_recv.at[chunk, rel, shift - 1], at_x(1)).wait_recv()
 
-    def xb_start():
-        block = wb.at[chip]
-        for shift in (1, 3, 2):
-            begin(move(block, xb_send.at[shift - 1], xb_recv.at[shift - 1], at_x(shift)))
-
-    def xb_wait(shift):
-        block = wb.at[index_of(0, NX - shift)]
-        move(block, xb_send.at[shift - 1], xb_recv.at[shift - 1], at_x(1)).wait_recv()
-
-    def zb_start(origin, step, column):
-        rel = (origin - step) % NZ
-        block = wb.at[index_of(origin, column)]
-        begin(move(block, zb_send.at[rel, column], zb_recv.at[rel, column], at_z(step)))
-
-    def zb_wait(origin, column):
-        rel = origin % NZ
-        block = wb.at[index_of(origin, column)]
-        move(block, zb_send.at[rel, column], zb_recv.at[rel, column], at_z(1)).wait_recv()
-
     far = {4: ((-3, -1, -2), (-4, -3, -1, -2)), -4: ((4, 3, 1, 2), (3, 1, 2))}
-    spread = (4, -4, 1, -1, 2, -2, 3, -3)
 
     for chunk in range(3):
+        for step in (4, -4, 3, -3, 1, -1, 2, -2):
+            zh_start(chunk, step)
         local(chunk).start()
         pair(chunk).start()
-    for chunk in range(2):
-        local(chunk).wait()
-        pair(chunk).wait_recv()
-        for step in spread:
-            za_start(chunk, 0, step)
-    local(2).wait()
-    pair(2).wait_recv()
-    xb_start()
-    for chunk in range(2):
-        xa_start(chunk, 0)
-    for step in spread:
-        zb_start(0, step, 0)
 
     def nb_copy(b):
         return pltpu.make_async_remote_copy(
@@ -203,24 +200,26 @@
         fetch.wait()
     lax.fori_loop(0, batch, norm_step, 0)
 
+    for chunk in range(3):
+        local(chunk).wait()
+        pair(chunk).wait_recv()
+        xa_start(chunk, 0)
     for origin in (1, -1, 2, -2):
-        for chunk in range(2):
-            za_wait(chunk, origin)
+        for chunk in range(3):
+            zh_wait(chunk, origin)
             xa_start(chunk, origin)
     for origin in (4, -4):
-        for chunk in range(2):
-            za_wait(chunk, origin)
-            for step in far[origin][chunk]:
+        for chunk in range(3):
+            zh_wait(chunk, origin)
+            for step in far[origin][chunk % 2]:
                 za_start(chunk, origin, step)
+    for origin in (3, -3):
+        for chunk in range(3):
+            zh_wait(chunk, origin)
             xa_start(chunk, origin)
-    for origin in (3, -3):
-        for chunk in range(2):
-            za_wait(chunk, origin)
+    for origin in (4, -4):
+        for chunk in range(3):
             xa_start(chunk, origin)
-    for shift in (1, 3, 2):
-        xb_wait(shift)
-        for step in spread:
-            zb_start(0, step, NX - shift)
 
     head = mine * 2 + core
     heads = 2 * tp
@@ -245,32 +244,21 @@
     lax.fori_loop(0, 2, bias_step, 0)
 
     late = (5, -5, 6, -6, 7, -7, 8)
-    for origin in (4, -4):
-        zb_wait(origin, 0)
-        for step in far[origin][0]:
-            zb_start(origin, step, 0)
     for origin in late:
-        za_wait(0, origin)
-        xa_start(0, origin)
-    for column in (3, 1, 2):
-        for origin in (4, -4):
-            zb_wait(origin, column)
-            for step in far[origin][column % 2]:
-                zb_start(origin, step, column)
-    for origin in late:
-        za_wait(1, origin)
-        xa_start(1, origin)
+        for chunk in range(3):
+            za_wait(chunk, origin)
+            xa_start(chunk, origin)
 
     lane = lax.broadcasted_iota(jnp.int32, (rows, 128), 1)
     low = lane < 64
     origins = (0, 1, -1, 2, -2, 3, -3, 4, -4) + late
 
-    def all_keys(chunk):
+    def all_blocks(chunk):
         for origin in origins:
             for shift in (1, 3, 2):
                 xa_wait(chunk, origin, shift)
 
-    all_keys(0)
+    all_blocks(0)
     wk2[...] = w2[...].reshape(wk2.shape)
     for b in range(batch):
         nb_copy(b).wait_recv()
@@ -316,13 +304,11 @@
         return step
 
     lax.fori_loop(0, batch, kv_step(wk2, (2,)), 0)
-    all_keys(1)
+    all_blocks(1)
     wk01[...] = w01[...].reshape(wk01.shape)
     lax.fori_loop(0, batch, kv_step(wk01, (0, 1)), 0)
 
-    for origin in (1, -1, 2, -2, 3, -3) + late:
-        for column in range(NX):
-            zb_wait(origin, column)
+    all_blocks(2)
     wq[...] = wb[...].reshape(wq.shape)
 
     tile = wq[:, 128:].astype(jnp.float32)
@@ -533,14 +519,12 @@
             dma((3,)),
             dma((3,)),
             dma((3,)),
-            dma((2, NZ)),
-            dma((2, NZ)),
-            dma((2, NZ, 3)),
-            dma((2, NZ, 3)),
-            dma((NZ, NX)),
-            dma((NZ, NX)),
-            dma((3,)),
-            dma((3,)),
+            dma((3, NZ, 2)),
+            dma((3, NZ, 2)),
+            dma((3, NZ)),
+            dma((3, NZ)),
+            dma((3, NZ, 3)),
+            dma((3, NZ, 3)),
             dma((batch,)),
             dma((batch,)),
             dma((batch, groups, 2)),

time: 63.9 us -> 66.8 us (1.045)
  the two profiles are of different devices: /device:TPU:96 before, /device:TPU:1 now
where the time goes in v3:
time: 66.8 us; the launch traced here: 66.7 us
  Pallas kernels  65 us (97%)
  local copies, waits for them, and re-layouts  1.67 us (2%)
    pallas_call x1, Pallas kernels, body(): pl.pallas_call(functools.partial(layer_kernel, tp, batch, length), out_sh...  65 us
    unnamed x1, local copies, waits for them, and re-layouts  1.67 us

profile of v3, /device:TPU:1, one launch (start us, length us, event | category | flops | bytes accessed | tf_op | source)
XLA Modules:
  0.0 66.7 jit_solution(1873023345476054861)
XLA Ops:
  0.0 65.0 %layer.1 = bf16[4,128,256]{2,1,0:T(8,128)(2,1)} custom-call(bf16[4,128,1024]{2,1,0:T(8,128)(2,1)} %x_hbm.1, f32[1,1024]{1,0:T(1,128)} %bitcast.2, bf16[8,3,2,64]{3,2,1,0:T(2,128)(2,1)} %qw_hbm.1, bf16[8,3,2,64]{3,2,1,0:T(2,128)(2,1)} %kw_hbm.1, bf16[8,3,2,64]{3,2,1,0:T(2,128)(2,1)} %vw_hbm.1, bf16[2,8,64]{2,1,0:T(8,128)(2,1)} %bitcast.3, f32[3,64]{1,0:T(4,128)} %qg_hbm.1, ...), custom_call_target="tpu_custom_call" | custom-call | tf_op jit(solution)/shard_map/layer/pallas_call | solution.py:492
  65.0 1.7 %copy.10 = bf16[4,128,256]{2,1,0:T(8,128)(2,1)} copy(bf16[4,128,256]{2,1,0:T(8,128)(2,1)} %layer.1) | data formatting | bytes 524288

commit v4 on v3

v4 whole, which is shorter than its diff:
```python
import functools
import math

import jax
import jax.numpy as jnp
from jax import lax
from jax.experimental import pallas as pl
from jax.experimental.pallas import tpu as pltpu
from jax.sharding import PartitionSpec as P

FOLDED = (1, 2)
GAPS = ((1, 32), (4, 32), (16, 16))
REACH = tuple(d * h for d, h in GAPS)
EPS = 1e-06
NEG = -1e30
LOG2E = 1.4426950408889634
MESH = pl.DeviceIdType.MESH
NZ, NX = 16, 4
CHIPS = NZ * NX
WB = 256


def layer_kernel(
    tp, batch, length, x_hbm, gain_hbm, qw_hbm, kw_hbm, vw_hbm, ow_hbm, qg_hbm, kg_hbm, out_ref,
    x_ref, gain_ref, qw_ref, kw_ref, vw_ref, ow_ref, qg_ref, kg_ref, slab_ref,
    w2, w01, wb, wk, wq, nb, win0, win1, win2, qn, bias0, bias1, bias2, osum, oown, orecv, wo, mboth, mrecv, mg,
    in_sem, pair_send, pair_recv, local_sem, out_sem, zh_recv, xh_recv, za_recv, xa_recv,
    nb_send, nb_recv, halo_send, halo_recv,
    o_send, o_recv, oy_send, oy_recv, m_send, m_recv, y_send, y_recv,
):
    me = lax.axis_index("sp")
    mine = lax.axis_index("tp")
    groups = len(GAPS)
    core = me % 2
    other = 1 - core
    chip = me // 2
    x = chip % NX
    z = chip // NX
    rows = 2 * length
    wins = (win0, win1, win2)
    biases = (bias0, bias1, bias2)
    bufs = (w2, w01, wb)

    def at_z(offset, on=core):
        return {"sp": (((z + offset + NZ) % NZ) * NX + x) * 2 + on}

    def at_x(offset, on=core):
        return {"sp": (z * NX + (x + offset) % NX) * 2 + on}

    sibling = {"sp": chip * 2 + other}

    def at_chip(offset):
        return {"sp": ((chip + offset + CHIPS) % CHIPS) * 2 + core}

    def at_y(offset):
        return {"tp": (mine + offset) % tp}

    barrier = pltpu.get_barrier_semaphore()

    def greet(target):
        pl.semaphore_signal(barrier, inc=1, device_id=target, device_id_type=MESH)

    targets = [at_z(o) for o in (-4, 4, -3, 3, -2, 2, -1, 1)] + [at_y(o) for o in range(1, tp)]
    targets += [at_x(o) for o in range(1, NX)] + [at_chip(1), at_chip(-1), sibling]
    targets += [at_x(2, other)]
    targets += [at_z(o, other) for o in (-4, 4, -3, 3, -2, 2, -1, 1)]
    for target in targets:
        greet(target)

    fetches = [
        pltpu.make_async_copy(src, dst, in_sem.at[i])
        for i, (src, dst) in enumerate(
            (
                (qw_hbm, qw_ref),
                (kw_hbm, kw_ref),
                (vw_hbm, vw_ref),
                (ow_hbm, ow_ref),
                (qg_hbm, qg_ref),
                (kg_hbm, kg_ref),
                (gain_hbm, gain_ref),
                (x_hbm, x_ref),
            )
        )
    ]
    for fetch in fetches:
        fetch.start()
    for fetch in fetches[:4]:
        fetch.wait()
    for head in range(2):
        pieces = []
        for group in (2, 0, 1):
            pieces += [kw_ref[:, group, head, :], vw_ref[:, group, head, :]]
        pieces += [qw_ref[:, group, head, :] for group in range(groups)]
        pieces = [piece.astype(jnp.float32) for piece in pieces + [ow_ref[head]]]
        slab_ref[head] = jnp.concatenate(pieces, axis=1).astype(jnp.bfloat16)

    pl.semaphore_wait(barrier, len(targets))

    cuts = (pl.ds(0, 128), pl.ds(128, 256), pl.ds(384, WB))

    def pair(chunk):
        return pltpu.make_async_remote_copy(
            src_ref=slab_ref.at[other, :, cuts[chunk]],
            dst_ref=bufs[chunk].at[chip, core],
            send_sem=pair_send.at[chunk],
            recv_sem=pair_recv.at[chunk],
            device_id=sibling,
            device_id_type=MESH,
        )

    def local(chunk):
        return pltpu.make_async_copy(
            slab_ref.at[core, :, cuts[chunk]], bufs[chunk].at[chip, core], local_sem.at[chunk]
        )

    def index_of(origin, column):
        return ((z + origin + NZ) % NZ) * NX + (x + column) % NX

    def move(block, send_sem, recv_sem, target, land=None):
        return pltpu.make_async_remote_copy(
            src_ref=block,
            dst_ref=block if land is None else land,
            send_sem=send_sem,
            recv_sem=recv_sem,
            device_id=target,
            device_id_type=MESH,
        )

    def zh_start(chunk, step):
        for on in (core, other):
            move(
                slab_ref.at[on, :, cuts[chunk]],
                out_sem.at[chunk],
                zh_recv.at[chunk, 3 - step if step < 0 else step - 1],
                at_z(step, on),
                bufs[chunk].at[chip, core],
            ).start()

    def zh_wait(chunk, origin):
        block = bufs[chunk].at[index_of(origin, 0)]
        slot = 3 + origin if origin > 0 else -origin - 1
        move(block, out_sem.at[chunk], zh_recv.at[chunk, slot], at_z(1)).wait_recv()

    def xh_start(chunk):
        for on in (core, other):
            move(
                slab_ref.at[on, :, cuts[chunk]],
                out_sem.at[chunk],
                xh_recv.at[chunk],
                at_x(2, on),
                bufs[chunk].at[chip, core],
            ).start()

    def xh_wait(chunk):
        move(bufs[chunk].at[index_of(0, 2)], out_sem.at[chunk], xh_recv.at[chunk], at_x(1)).wait_recv()

    def slot_of(rel, fold):
        if fold == 0:
            return rel - 5
        return {4: 7, NZ - 4: 8}.get(rel, 9)

    def za_start(chunk, origin, step, fold=0):
        slot = slot_of((origin - step) % NZ, fold)
        block = bufs[chunk].at[index_of(origin, 2 * fold)]
        move(block, out_sem.at[chunk], za_recv.at[chunk, slot], at_z(step)).start()

    def za_wait(chunk, origin, fold=0):
        block = bufs[chunk].at[index_of(origin, 2 * fold)]
        move(block, out_sem.at[chunk], za_recv.at[chunk, slot_of(origin % NZ, fold)], at_z(1)).wait_recv()

    def shifts(chunk):
        return (1, 3) if chunk in FOLDED else (1, 3, 2)

    def xa_start(chunk, origin):
        block = bufs[chunk].at[index_of(origin, 0)]
        for shift in shifts(chunk):
            move(block, out_sem.at[chunk], xa_recv.at[chunk], at_x(shift)).start()

    far = {4: ((-3, -1, -2), (-4, -3, -1, -2)), -4: ((4, 3, 1, 2), (3, 1, 2))}

    for step in (4, -4, 3, -3, 1, -1, 2, -2):
        zh_start(0, step)
    for steps in ((4, -4), (1, -1, 2, -2, 3, -3)):
        for chunk in (1, 2):
            for step in steps:
                zh_start(chunk, step)
    for chunk in FOLDED:
        xh_start(chunk)
    for chunk in range(3):
        local(chunk).start()
        pair(chunk).start()

    def nb_copy(b):
        return move(nb.at[b, core], nb_send.at[0], nb_recv.at[0], sibling)

    def norm_step(b, carry):
        flat = x_ref[b].astype(jnp.float32)
        scale = lax.rsqrt(jnp.mean(flat * flat, axis=-1, keepdims=True) + EPS)
        nb[b, core] = (flat * scale * gain_ref[...]).astype(jnp.bfloat16)
        nb_copy(b).start()
        return carry

    for fetch in fetches[4:]:
        fetch.wait()
    lax.fori_loop(0, batch, norm_step, 0)

    for chunk in range(3):
        local(chunk).wait()
        pair(chunk).wait_recv()
        xa_start(chunk, 0)

    def near(chunk, spread):
        for origin in (1, -1, 2, -2):
            zh_wait(chunk, origin)
            if spread:
                xa_start(chunk, origin)
        for origin in (4, -4):
            zh_wait(chunk, origin)
            for step in far[origin][chunk % 2]:
                za_start(chunk, origin, step)
        for origin in (3, -3):
            zh_wait(chunk, origin)
            if spread:
                xa_start(chunk, origin)
        if spread:
            for origin in (4, -4):
                xa_start(chunk, origin)

    near(0, True)
    for chunk in FOLDED:
        xh_wait(chunk)
        for step in (4, -4, 3, -3, 1, -1, 2, -2):
            za_start(chunk, 0, step, 1)
    near(1, True)
    near(2, True)

    head = mine * 2 + core
    heads = 2 * tp
    power = -8.0 * (head + 1).astype(jnp.float32) / heads
    slope = jnp.exp2(jnp.full((8, 128), power, jnp.float32))[:1, :1] * LOG2E
    total_rows = CHIPS * rows

    def bias_of(group, count, first):
        dilation, half = GAPS[group]
        reach = REACH[group]
        shape = (count, count + 2 * reach)
        key = lax.broadcasted_iota(jnp.int32, shape, 1) - reach
        offset = jnp.abs(key - lax.broadcasted_iota(jnp.int32, shape, 0))
        at = key + (chip * rows + first)
        allowed = (offset <= reach) & (at >= 0) & (at < total_rows) & ((offset & (dilation - 1)) == 0)
        return jnp.where(allowed, offset.astype(jnp.float32) * (-slope / float(reach)), NEG)

    for block in range(2):
        bias0[block] = bias_of(0, length, block * length)
    for group in (1, 2):
        biases[group][...] = bias_of(group, rows, 0)

    late = (5, -5, 6, -6, 7, -7, 8)
    def fold_on(chunk):
        for origin in (4, -4):
            za_wait(chunk, origin, 1)
            for step in far[origin][1 - chunk % 2]:
                za_start(chunk, origin, step, 1)

    def late_on(chunk, part):
        for origin in part:
            za_wait(chunk, origin)
            xa_start(chunk, origin)

    late_on(0, late[:4])
    fold_on(1)
    late_on(0, late[4:])
    fold_on(2)
    late_on(1, late)
    late_on(2, late)

    lane = lax.broadcasted_iota(jnp.int32, (rows, 128), 1)
    low = lane < 64
    origins = (0, 1, -1, 2, -2, 3, -3, 4, -4) + late

    def all_blocks(chunk):
        several = bufs[chunk].at[pl.ds(0, NZ * len(shifts(chunk)))]
        move(several, out_sem.at[chunk], xa_recv.at[chunk], at_x(1)).wait_recv()
        if chunk in FOLDED:
            several = bufs[chunk].at[pl.ds(0, NZ - 3)]
            move(several, out_sem.at[chunk], za_recv.at[chunk, 9], at_x(1)).wait_recv()

    all_blocks(0)
    wk[:, :128] = w2[...].reshape(wk.shape[0], 128)
    nb_all = move(nb.at[:, 0], nb_send.at[0], nb_recv.at[0], sibling)
    nb_all.wait_recv()

    def halo(b, group, up):
        reach = REACH[group]
        begin_at, land_at = (rows, 0) if up else (reach, reach + rows)
        return pltpu.make_async_remote_copy(
            src_ref=wins[group].at[b, pl.ds(begin_at, reach), :],
            dst_ref=wins[group].at[b, pl.ds(land_at, reach), :],
            send_sem=halo_send.at[group],
            recv_sem=halo_recv.at[b, group],
            device_id=at_chip(1 if up else -1),
            device_id_type=MESH,
        )

    def halo_wait(b):
        for group in (2, 1, 0):
            both = wins[group].at[b, pl.ds(0, 2 * REACH[group]), :]
            move(both, halo_send.at[group], halo_recv.at[b, group], at_chip(1)).wait_recv()

    ones = jnp.ones((1, 64), jnp.float32)
    zeros = jnp.zeros((1, 64), jnp.float32)

    def key_norm(out, place, group):
        seg = out[:, 128 * place : 128 * (place + 1)].astype(jnp.bfloat16).astype(jnp.float32)
        mean = jnp.sum(jnp.where(low, seg * seg, 0.0), axis=-1, keepdims=True) / 64.0
        gain = jnp.concatenate([kg_ref[group : group + 1, :], ones], axis=1)
        return (seg * jnp.where(low, lax.rsqrt(mean + EPS), 1.0) * gain).astype(jnp.bfloat16)

    def key_step(b, first, order):
        out = jnp.dot(nb[b].reshape(rows, -1), wk[:, first : first + 128 * len(order)], preferred_element_type=jnp.float32)
        for place, group in enumerate(order):
            wins[group][b, REACH[group] : REACH[group] + rows, :] = key_norm(out, place, group)
        for group in order:
            for up in (True, False):
                halo(b, group, up).start()

    for b in range(batch):
        key_step(b, 0, (2,))
    all_blocks(1)
    wk[:, 128:] = w01[...].reshape(wk.shape[0], 256)
    for b in range(batch):
        key_step(b, 128, (0, 1))

    all_blocks(2)
    wq[...] = wb[...].reshape(wq.shape)

    tile = wq[:, 128:].astype(jnp.float32)
    high = lax.broadcasted_iota(jnp.int32, tile.shape, 1) >= 64
    tile = jnp.where(high, tile, 0.0)
    tile = jnp.where(core == 0, pltpu.roll(tile, 64, 1), tile)
    oown[...] = tile.astype(jnp.bfloat16)
    o_pair = pltpu.make_async_remote_copy(
        src_ref=oown,
        dst_ref=orecv,
        send_sem=o_send.at[0],
        recv_sem=o_recv.at[0],
        device_id=sibling,
        device_id_type=MESH,
    )
    o_pair.start()

    factor = LOG2E / 8.0

    def q_step(b, carry):
        out = jnp.dot(nb[b].reshape(rows, -1), wq[...], preferred_element_type=jnp.float32)
        out = out.astype(jnp.bfloat16).astype(jnp.float32)
        first, second = out[:, :128], out[:, 128:]
        for group, seg, here in ((0, first, low), (1, first, ~low), (2, second, low)):
            mean = jnp.sum(jnp.where(here, seg * seg, 0.0), axis=-1, keepdims=True) / 64.0
            gain = qg_ref[group : group + 1, :] * factor
            gain = jnp.concatenate([zeros, gain] if group == 1 else [gain, zeros], axis=1)
            scaled = jnp.where(here, seg * lax.rsqrt(mean + EPS) * gain, 0.0)
            if group == 1:
                scaled = pltpu.roll(scaled, 64, 1)
            qn[group, b] = scaled.astype(jnp.bfloat16)
        return carry

    for i in range(batch):
        q_step(i, 0)

    span = wo.shape[1]
    o_pair.wait_recv()
    osum[...] = (oown[...] + orecv[...]).reshape(osum.shape)
    wo[mine] = osum[mine]

    def o_copy(shift):
        return move(osum.at[(mine + shift) % tp], oy_send.at[0], oy_recv.at[0], at_y(shift), wo.at[mine])

    o_all = move(wo.at[pl.ds(0, tp - 1)], oy_send.at[0], oy_recv.at[0], at_y(1))

    for shift in range(1, tp):
        o_copy(shift).start()

    keep = lane >= 64

    def attend(b):
        total = jnp.zeros((rows, 1), jnp.float32)
        summed = jnp.zeros((rows, 128), jnp.float32)
        for group in (2, 1):
            window = wins[group][b]
            scores = lax.dot_general(
                qn[group, b], window, (((1,), (1,)), ((), ())), preferred_element_type=jnp.float32
            )
            grown = jnp.exp2(scores + biases[group][...])
            total = total + jnp.sum(grown, axis=-1, keepdims=True)
            summed = summed + jnp.dot(grown.astype(jnp.bfloat16), window, preferred_element_type=jnp.float32)
        close = length + 2 * REACH[0]
        totals, sums = [], []
        for block in range(2):
            window = win0[b, block * length : block * length + close, :]
            query = qn[0, b, block * length : (block + 1) * length, :]
            scores = lax.dot_general(query, window, (((1,), (1,)), ((), ())), preferred_element_type=jnp.float32)
            grown = jnp.exp2(scores + bias0[block])
            totals.append(jnp.sum(grown, axis=-1, keepdims=True))
            sums.append(jnp.dot(grown.astype(jnp.bfloat16), window, preferred_element_type=jnp.float32))
        total = total + jnp.concatenate(totals, axis=0)
        summed = summed + jnp.concatenate(sums, axis=0)
        merged = jnp.where(keep, summed / total, 0.0)
        merged = jnp.where(core == 0, pltpu.roll(merged, 64, 1), merged).astype(jnp.bfloat16)
        mboth[b] = merged.reshape(2, length, 128)

    def m_copy(b):
        return move(mboth.at[b, other], m_send.at[0], m_recv.at[b], sibling, mrecv.at[b])

    def y_copy(b, shift):
        return move(mg.at[mine, b], y_send.at[0], y_recv.at[b], at_y(shift))

    def y_wait(b):
        move(mg.at[pl.ds(0, tp - 1), b], y_send.at[0], y_recv.at[b], at_y(1)).wait_recv()

    def pass_on(b):
        m_copy(b).wait_recv()
        mg[mine, b] = mboth[b, core] + mrecv[b]
        for shift in range(1, tp):
            y_copy(b, shift).start()

    def attend_step(i, carry):
        b = i
        halo_wait(b)
        attend(b)
        m_copy(b).start()

        @pl.when(i >= 1)
        def _():
            pass_on(i - 1)

        return carry

    lax.fori_loop(0, batch, attend_step, 0)
    pass_on(batch - 1)
    o_all.wait_recv()

    def finish(b, carry):
        y_wait(b)
        final = jnp.zeros((length, span), jnp.float32)
        for part in range(tp):
            final = final + lax.dot_general(
                mg[part, b], wo[part], (((1,), (1,)), ((), ())), preferred_element_type=jnp.float32
            )
        out_ref[b] = final.astype(jnp.bfloat16)
        return carry

    lax.fori_loop(0, batch, finish, 0)
    for chunk in range(3):
        pair(chunk).wait_send()
        sent = bufs[chunk].at[pl.ds(0, CHIPS - 1)]
        move(sent, out_sem.at[chunk], xa_recv.at[chunk], at_x(1)).wait_send()
    nb_all.wait_send()
    for group in range(groups):
        both = wins[group].at[:, pl.ds(0, 2 * REACH[group]), :]
        move(both, halo_send.at[group], halo_recv.at[0, group], at_chip(1)).wait_send()
    o_pair.wait_send()
    o_all.wait_send()
    move(mrecv, m_send.at[0], m_recv.at[0], sibling).wait_send()
    move(mg.at[pl.ds(0, tp - 1)], y_send.at[0], y_recv.at[0], at_y(1)).wait_send()


def body(tp, inputs, norm_gain, query_weight, key_weight, value_weight, query_gain, key_gain, out_weight):
    batch, length, model = inputs.shape
    share, groups, heads, width = query_weight.shape
    span = model // tp
    rows = 2 * length
    bf16 = jnp.bfloat16
    dma = pltpu.SemaphoreType.DMA
    operands = (
        inputs,
        norm_gain.reshape(1, model),
        query_weight,
        key_weight,
        value_weight,
        out_weight.transpose(0, 2, 1),
        query_gain,
        key_gain,
    )
    return pl.pallas_call(
        functools.partial(layer_kernel, tp, batch, length),
        out_shape=jax.ShapeDtypeStruct((batch, length, span), bf16),
        in_specs=[pl.BlockSpec(memory_space=pl.ANY)] * len(operands),
        out_specs=pl.BlockSpec(memory_space=pltpu.VMEM),
        scratch_shapes=[
            *[pltpu.VMEM(operand.shape, operand.dtype) for operand in operands],
            pltpu.VMEM((heads, share, 384 + WB), bf16),
            pltpu.VMEM((CHIPS, 2, share, 128), bf16),
            pltpu.VMEM((CHIPS, 2, share, 256), bf16),
            pltpu.VMEM((CHIPS, 2, share, WB), bf16),
            pltpu.VMEM((model, 384), bf16),
            pltpu.VMEM((model, WB), bf16),
            pltpu.VMEM((batch, 2, length, model), bf16),
            *[pltpu.VMEM((batch, rows + 2 * r, 128), bf16) for r in REACH],
            pltpu.VMEM((groups, batch, rows, 128), bf16),
            pltpu.VMEM((2, length, length + 2 * REACH[0]), jnp.float32),
            *[pltpu.VMEM((rows, rows + 2 * r), jnp.float32) for r in REACH[1:]],
            pltpu.VMEM((tp, span, 128), bf16),
            pltpu.VMEM((model, 128), bf16),
            pltpu.VMEM((model, 128), bf16),
            pltpu.VMEM((tp, span, 128), bf16),
            pltpu.VMEM((batch, 2, length, 128), bf16),
            pltpu.VMEM((batch, length, 128), bf16),
            pltpu.VMEM((tp, batch, length, 128), bf16),
            dma((len(operands),)),
            dma((3,)),
            dma((3,)),
            dma((3,)),
            dma((3,)),
            dma((3, 8)),
            dma((3,)),
            dma((3, 10)),
            dma((3,)),
            dma((1,)),
            dma((1,)),
            dma((groups,)),
            dma((batch, groups)),
            dma((1,)),
            dma((1,)),
            dma((1,)),
            dma((1,)),
            dma((1,)),
            dma((batch,)),
            dma((1,)),
            dma((batch,)),
        ],
        compiler_params=pltpu.CompilerParams(collective_id=0, has_side_effects=True, vmem_limit_bytes=60 * 1024 * 1024),
        name="layer",
    )(*operands)


def solution(mesh):
    in_specs = (
        P(None, "sp", None),
        P(),
        P("sp", None, "tp", None),
        P("sp", None, "tp", None),
        P("sp", None, "tp", None),
        P(),
        P(),
        P("tp", None, "sp"),
    )
    out_specs = P(None, "sp", "tp")
    run = functools.partial(body, mesh.shape["tp"])
    return jax.shard_map(run, mesh=mesh, in_specs=in_specs, out_specs=out_specs, check_vma=False)
```

time: 66.8 us -> 60.7 us (0.909)
  Pallas kernels: 65 us -> 58.9 us
    pallas_call x1, Pallas kernels: 65 us -> 58.9 us  [body(): pl.pallas_call(functools.partial(layer_kernel, tp, batch, length), out_sh...]
where the time goes in v4:
time: 60.7 us; the launch traced here: 60.5 us
  Pallas kernels  58.9 us (97%)
  local copies, waits for them, and re-layouts  1.67 us (3%)
    pallas_call x1, Pallas kernels, body(): pl.pallas_call(functools.partial(layer_kernel, tp, batch, length), out_sh...  58.9 us
    unnamed x1, local copies, waits for them, and re-layouts  1.67 us

profile of v4, /device:TPU:1, one launch (start us, length us, event | category | flops | bytes accessed | tf_op | source)
XLA Modules:
  0.0 60.5 jit_solution(11970329120920632528)
XLA Ops:
  0.0 58.9 %layer.1 = bf16[4,128,256]{2,1,0:T(8,128)(2,1)} custom-call(bf16[4,128,1024]{2,1,0:T(8,128)(2,1)} %x_hbm.1, f32[1,1024]{1,0:T(1,128)} %bitcast.2, bf16[8,3,2,64]{3,2,1,0:T(2,128)(2,1)} %qw_hbm.1, bf16[8,3,2,64]{3,2,1,0:T(2,128)(2,1)} %kw_hbm.1, bf16[8,3,2,64]{3,2,1,0:T(2,128)(2,1)} %vw_hbm.1, bf16[2,8,64]{2,1,0:T(8,128)(2,1)} %bitcast.3, f32[3,64]{1,0:T(4,128)} %qg_hbm.1, ...), custom_call_target="tpu_custom_call" | custom-call | tf_op jit(solution)/shard_map/layer/pallas_call | solution.py:485
  58.9 1.7 %copy.10 = bf16[4,128,256]{2,1,0:T(8,128)(2,1)} copy(bf16[4,128,256]{2,1,0:T(8,128)(2,1)} %layer.1) | data formatting | bytes 524288

commit v5 on v4

--- a/solution.py
+++ b/solution.py
@@ -8,7 +8,7 @@
 from jax.experimental.pallas import tpu as pltpu
 from jax.sharding import PartitionSpec as P
 
-FOLDED = (1, 2)
+FOLDED = (2,)
 GAPS = ((1, 32), (4, 32), (16, 16))
 REACH = tuple(d * h for d, h in GAPS)
 EPS = 1e-06
@@ -268,9 +268,9 @@
             xa_start(chunk, origin)
 
     late_on(0, late[:4])
-    fold_on(1)
+    for chunk in FOLDED:
+        fold_on(chunk)
     late_on(0, late[4:])
-    fold_on(2)
     late_on(1, late)
     late_on(2, late)
 
@@ -284,6 +284,9 @@
         if chunk in FOLDED:
             several = bufs[chunk].at[pl.ds(0, NZ - 3)]
             move(several, out_sem.at[chunk], za_recv.at[chunk, 9], at_x(1)).wait_recv()
+
+    def sent_all(chunk):
+        move(bufs[chunk].at[pl.ds(0, CHIPS - 1)], out_sem.at[chunk], xa_recv.at[chunk], at_x(1)).wait_send()
 
     all_blocks(0)
     wk[:, :128] = w2[...].reshape(wk.shape[0], 128)
@@ -321,12 +324,26 @@
         for place, group in enumerate(order):
             wins[group][b, REACH[group] : REACH[group] + rows, :] = key_norm(out, place, group)
         for group in order:
-            for up in (True, False):
-                halo(b, group, up).start()
+            halo(b, group, False).start()
+            if group == 2:
+
+                @pl.when(x != NX - 1)
+                def _():
+                    halo(b, 2, True).start()
+
+            else:
+                halo(b, group, True).start()
 
     for b in range(batch):
         key_step(b, 0, (2,))
     all_blocks(1)
+    sent_all(2)
+
+    @pl.when(x == NX - 1)
+    def _():
+        for b in range(batch):
+            halo(b, 2, True).start()
+
     wk[:, 128:] = w01[...].reshape(wk.shape[0], 256)
     for b in range(batch):
         key_step(b, 128, (0, 1))
@@ -381,33 +398,46 @@
     for shift in range(1, tp):
         o_copy(shift).start()
 
-    keep = lane >= 64
+    def merge(total, summed):
+        merged = jnp.where(lax.broadcasted_iota(jnp.int32, summed.shape, 1) >= 64, summed / total, 0.0)
+        return jnp.where(core == 0, pltpu.roll(merged, 64, 1), merged).astype(jnp.bfloat16)
+
+    def close_part(b, block):
+        begin = block * length if isinstance(block, int) else pl.multiple_of(block * length, length)
+        window = win0[b, pl.ds(begin, length + 2 * REACH[0]), :]
+        query = qn[0, b, pl.ds(begin, length), :]
+        scores = lax.dot_general(query, window, (((1,), (1,)), ((), ())), preferred_element_type=jnp.float32)
+        grown = jnp.exp2(scores + bias0[block])
+        total = jnp.sum(grown, axis=-1, keepdims=True)
+        return total, jnp.dot(grown.astype(jnp.bfloat16), window, preferred_element_type=jnp.float32)
+
+    def wide_part(b, group, begin, count):
+        window = wins[group][b, pl.ds(begin, count + 2 * REACH[group]), :]
+        query = qn[group, b, pl.ds(begin, count), :]
+        scores = lax.dot_general(query, window, (((1,), (1,)), ((), ())), preferred_element_type=jnp.float32)
+        first = begin if isinstance(begin, int) else pl.multiple_of(begin, length)
+        bias = biases[group][pl.ds(0, count), pl.ds(0, count + 2 * REACH[group])]
+        if count != rows:
+            bias = biases[group][pl.ds(first, count), pl.ds(first, count + 2 * REACH[group])]
+        grown = jnp.exp2(scores + bias)
+        total = jnp.sum(grown, axis=-1, keepdims=True)
+        return total, jnp.dot(grown.astype(jnp.bfloat16), window, preferred_element_type=jnp.float32)
 
     def attend(b):
-        total = jnp.zeros((rows, 1), jnp.float32)
-        summed = jnp.zeros((rows, 128), jnp.float32)
-        for group in (2, 1):
-            window = wins[group][b]
-            scores = lax.dot_general(
-                qn[group, b], window, (((1,), (1,)), ((), ())), preferred_element_type=jnp.float32
-            )
-            grown = jnp.exp2(scores + biases[group][...])
-            total = total + jnp.sum(grown, axis=-1, keepdims=True)
-            summed = summed + jnp.dot(grown.astype(jnp.bfloat16), window, preferred_element_type=jnp.float32)
-        close = length + 2 * REACH[0]
-        totals, sums = [], []
-        for block in range(2):
-            window = win0[b, block * length : block * length + close, :]
-            query = qn[0, b, block * length : (block + 1) * length, :]
-            scores = lax.dot_general(query, window, (((1,), (1,)), ((), ())), preferred_element_type=jnp.float32)
-            grown = jnp.exp2(scores + bias0[block])
-            totals.append(jnp.sum(grown, axis=-1, keepdims=True))
-            sums.append(jnp.dot(grown.astype(jnp.bfloat16), window, preferred_element_type=jnp.float32))
-        total = total + jnp.concatenate(totals, axis=0)
-        summed = summed + jnp.concatenate(sums, axis=0)
-        merged = jnp.where(keep, summed / total, 0.0)
-        merged = jnp.where(core == 0, pltpu.roll(merged, 64, 1), merged).astype(jnp.bfloat16)
-        mboth[b] = merged.reshape(2, length, 128)
+        total, summed = wide_part(b, 2, 0, rows)
+        for part_total, part_sum in [
+            wide_part(b, 1, 0, rows),
+            [jnp.concatenate(both, axis=0) for both in zip(close_part(b, 0), close_part(b, 1))],
+        ]:
+            total, summed = total + part_total, summed + part_sum
+        mboth[b] = merge(total, summed).reshape(2, length, 128)
+
+    def attend_block(b, block):
+        begin = pl.multiple_of(block * length, length)
+        total, summed = wide_part(b, 2, begin, length)
+        for part_total, part_sum in (wide_part(b, 1, begin, length), close_part(b, block)):
+            total, summed = total + part_total, summed + part_sum
+        mboth[b, block] = merge(total, summed)
 
     def m_copy(b):
         return move(mboth.at[b, other], m_send.at[0], m_recv.at[b], sibling, mrecv.at[b])
@@ -436,7 +466,13 @@
 
         return carry
 
-    lax.fori_loop(0, batch, attend_step, 0)
+    lax.fori_loop(0, batch - 1, attend_step, 0)
+    last = batch - 1
+    halo_wait(last)
+    attend_block(last, other)
+    m_copy(last).start()
+    pass_on(last - 1)
+    attend_block(last, core)
     pass_on(batch - 1)
     o_all.wait_recv()
 
@@ -453,8 +489,8 @@
     lax.fori_loop(0, batch, finish, 0)
     for chunk in range(3):
         pair(chunk).wait_send()
-        sent = bufs[chunk].at[pl.ds(0, CHIPS - 1)]
-        move(sent, out_sem.at[chunk], xa_recv.at[chunk], at_x(1)).wait_send()
+        if chunk < 2:
+            sent_all(chunk)
     nb_all.wait_send()
     for group in range(groups):
         both = wins[group].at[:, pl.ds(0, 2 * REACH[group]), :]

time: 60.7 us -> 56.1 us (0.924)
  Pallas kernels: 58.9 us -> 54.2 us
    pallas_call x1, Pallas kernels: 58.9 us -> 54.2 us  [body(): pl.pallas_call(functools.partial(layer_kernel, tp, batch, length), out_sh...]
where the time goes in v5:
time: 56.1 us; the launch traced here: 55.9 us
  Pallas kernels  54.2 us (97%)
  local copies, waits for them, and re-layouts  1.67 us (3%)
    pallas_call x1, Pallas kernels, body(): pl.pallas_call(functools.partial(layer_kernel, tp, batch, length), out_sh...  54.2 us
    unnamed x1, local copies, waits for them, and re-layouts  1.67 us

profile of v5, /device:TPU:1, one launch (start us, length us, event | category | flops | bytes accessed | tf_op | source)
XLA Modules:
  0.0 55.9 jit_solution(14600173866450856245)
XLA Ops:
  0.0 54.2 %layer.1 = bf16[4,128,256]{2,1,0:T(8,128)(2,1)} custom-call(bf16[4,128,1024]{2,1,0:T(8,128)(2,1)} %x_hbm.1, f32[1,1024]{1,0:T(1,128)} %bitcast.2, bf16[8,3,2,64]{3,2,1,0:T(2,128)(2,1)} %qw_hbm.1, bf16[8,3,2,64]{3,2,1,0:T(2,128)(2,1)} %kw_hbm.1, bf16[8,3,2,64]{3,2,1,0:T(2,128)(2,1)} %vw_hbm.1, bf16[2,8,64]{2,1,0:T(8,128)(2,1)} %bitcast.3, f32[3,64]{1,0:T(4,128)} %qg_hbm.1, ...), custom_call_target="tpu_custom_call" | custom-call | tf_op jit(solution)/shard_map/layer/pallas_call | solution.py:521
  54.2 1.7 %copy.10 = bf16[4,128,256]{2,1,0:T(8,128)(2,1)} copy(bf16[4,128,256]{2,1,0:T(8,128)(2,1)} %layer.1) | data formatting | bytes 524288

commit v6 on v5

--- a/solution.py
+++ b/solution.py
@@ -26,7 +26,7 @@
     w2, w01, wb, wk, wq, nb, win0, win1, win2, qn, bias0, bias1, bias2, osum, oown, orecv, wo, mboth, mrecv, mg,
     in_sem, pair_send, pair_recv, local_sem, out_sem, zh_recv, xh_recv, za_recv, xa_recv,
     nb_send, nb_recv, halo_send, halo_recv,
-    o_send, o_recv, oy_send, oy_recv, m_send, m_recv, y_send, y_recv,
+    o_send, o_recv, oy_send, oy_recv, m_send, m_recv, y_send, y_recv, outs, out_move,
 ):
     me = lax.axis_index("sp")
     mine = lax.axis_index("tp")
@@ -102,15 +102,15 @@
         return pltpu.make_async_remote_copy(
             src_ref=slab_ref.at[other, :, cuts[chunk]],
             dst_ref=bufs[chunk].at[chip, core],
-            send_sem=pair_send.at[chunk],
-            recv_sem=pair_recv.at[chunk],
+            send_sem=pair_send.at[0],
+            recv_sem=pair_recv.at[0],
             device_id=sibling,
             device_id_type=MESH,
         )
 
     def local(chunk):
         return pltpu.make_async_copy(
-            slab_ref.at[core, :, cuts[chunk]], bufs[chunk].at[chip, core], local_sem.at[chunk]
+            slab_ref.at[core, :, cuts[chunk]], bufs[chunk].at[chip, core], local_sem.at[0]
         )
 
     def index_of(origin, column):
@@ -204,9 +204,10 @@
         fetch.wait()
     lax.fori_loop(0, batch, norm_step, 0)
 
+    pair_all = move(slab_ref.at[0], pair_send.at[0], pair_recv.at[0], sibling)
+    pltpu.make_async_copy(slab_ref.at[0], slab_ref.at[1], local_sem.at[0]).wait()
+    pair_all.wait_recv()
     for chunk in range(3):
-        local(chunk).wait()
-        pair(chunk).wait_recv()
         xa_start(chunk, 0)
 
     def near(chunk, spread):
@@ -324,25 +325,27 @@
         for place, group in enumerate(order):
             wins[group][b, REACH[group] : REACH[group] + rows, :] = key_norm(out, place, group)
         for group in order:
-            halo(b, group, False).start()
-            if group == 2:
-
-                @pl.when(x != NX - 1)
-                def _():
-                    halo(b, 2, True).start()
-
-            else:
-                halo(b, group, True).start()
+            for up in (True, False):
+                if group == 2:
+
+                    @pl.when(x != (NX - 1 if up else 0))
+                    def _(up=up):
+                        halo(b, 2, up).start()
+
+                else:
+                    halo(b, group, up).start()
 
     for b in range(batch):
         key_step(b, 0, (2,))
     all_blocks(1)
     sent_all(2)
 
-    @pl.when(x == NX - 1)
-    def _():
-        for b in range(batch):
-            halo(b, 2, True).start()
+    for up in (True, False):
+
+        @pl.when(x == (NX - 1 if up else 0))
+        def _(up=up):
+            for b in range(batch):
+                halo(b, 2, up).start()
 
     wk[:, 128:] = w01[...].reshape(wk.shape[0], 256)
     for b in range(batch):
@@ -476,6 +479,9 @@
     pass_on(batch - 1)
     o_all.wait_recv()
 
+    def out_copy(b):
+        return pltpu.make_async_copy(outs.at[b], out_ref.at[b], out_move.at[0])
+
     def finish(b, carry):
         y_wait(b)
         final = jnp.zeros((length, span), jnp.float32)
@@ -483,14 +489,15 @@
             final = final + lax.dot_general(
                 mg[part, b], wo[part], (((1,), (1,)), ((), ())), preferred_element_type=jnp.float32
             )
-        out_ref[b] = final.astype(jnp.bfloat16)
+        outs[b] = final.astype(jnp.bfloat16)
+        out_copy(b).start()
         return carry
 
     lax.fori_loop(0, batch, finish, 0)
-    for chunk in range(3):
-        pair(chunk).wait_send()
-        if chunk < 2:
-            sent_all(chunk)
+    pltpu.make_async_copy(outs, out_ref, out_move.at[0]).wait()
+    pair_all.wait_send()
+    for chunk in range(2):
+        sent_all(chunk)
     nb_all.wait_send()
     for group in range(groups):
         both = wins[group].at[:, pl.ds(0, 2 * REACH[group]), :]
@@ -521,8 +528,8 @@
     return pl.pallas_call(
         functools.partial(layer_kernel, tp, batch, length),
         out_shape=jax.ShapeDtypeStruct((batch, length, span), bf16),
-        in_specs=[pl.BlockSpec(memory_space=pl.ANY)] * len(operands),
-        out_specs=pl.BlockSpec(memory_space=pltpu.VMEM),
+        in_specs=[pl.BlockSpec(memory_space=pltpu.HBM)] * len(operands),
+        out_specs=pl.BlockSpec(memory_space=pl.ANY),
         scratch_shapes=[
             *[pltpu.VMEM(operand.shape, operand.dtype) for operand in operands],
             pltpu.VMEM((heads, share, 384 + WB), bf16),
@@ -544,9 +551,9 @@
             pltpu.VMEM((batch, length, 128), bf16),
             pltpu.VMEM((tp, batch, length, 128), bf16),
             dma((len(operands),)),
-            dma((3,)),
-            dma((3,)),
-            dma((3,)),
+            dma((1,)),
+            dma((1,)),
+            dma((1,)),
             dma((3,)),
             dma((3, 8)),
             dma((3,)),
@@ -564,10 +571,12 @@
             dma((batch,)),
             dma((1,)),
             dma((batch,)),
+            pltpu.VMEM((batch, length, span), bf16),
+            dma((1,)),
         ],
-        compiler_params=pltpu.CompilerParams(collective_id=0, has_side_effects=True, vmem_limit_bytes=60 * 1024 * 1024),
+        compiler_params=pltpu.CompilerParams(collective_id=0, has_side_effects=True, vmem_limit_bytes=24 * 1024 * 1024),
         name="layer",
-    )(*operands)
+    )(*[pltpu.with_memory_space_constraint(operand, pltpu.HBM) for operand in operands])
 
 
 def solution(mesh):

time: 56.1 us -> 54.4 us (0.970)
  local copies, waits for them, and re-layouts: 1.67 us -> 0.71 us
  Pallas kernels: 54.2 us -> 53.5 us
    unnamed x1, local copies, waits for them, and re-layouts: 1.67 us -> 0.71 us
    pallas_call x1, Pallas kernels: 54.2 us -> 53.5 us  [body(): pl.pallas_call(functools.partial(layer_kernel, tp, batch, length), out_sh...]
where the time goes in v6:
time: 54.4 us; the launch traced here: 54.3 us
  Pallas kernels  53.5 us (98%)
  local copies, waits for them, and re-layouts  0.71 us (1%)
    pallas_call x1, Pallas kernels, body(): pl.pallas_call(functools.partial(layer_kernel, tp, batch, length), out_sh...  53.5 us

profile of v6, /device:TPU:1, one launch (start us, length us, event | category | flops | bytes accessed | tf_op | source)
XLA Modules:
  0.0 54.3 jit_solution(4882943723435364141)
XLA Ops:
  0.0 53.5 %layer.1 = bf16[4,128,256]{2,1,0:T(8,128)(2,1)S(1)} custom-call(bf16[4,128,1024]{2,1,0:T(8,128)(2,1)} %x_hbm.1, f32[1,1024]{1,0:T(1,128)} %bitcast.2, bf16[8,3,2,64]{3,2,1,0:T(2,128)(2,1)} %qw_hbm.1, bf16[8,3,2,64]{3,2,1,0:T(2,128)(2,1)} %kw_hbm.1, bf16[8,3,2,64]{3,2,1,0:T(2,128)(2,1)} %vw_hbm.1, bf16[2,8,64]{2,1,0:T(8,128)(2,1)} %bitcast.3, ...), custom_call_target="tpu_custom_call" | custom-call | tf_op jit(solution)/shard_map/layer/pallas_call | solution.py:528
  53.6 0.7 %copy.10 = bf16[4,128,256]{2,1,0:T(8,128)(2,1)} copy(bf16[4,128,256]{2,1,0:T(8,128)(2,1)S(1)} %layer.1) | data formatting | bytes 524288

commit v7 on v6

--- a/solution.py
+++ b/solution.py
@@ -169,7 +169,7 @@
         move(block, out_sem.at[chunk], za_recv.at[chunk, slot_of(origin % NZ, fold)], at_z(1)).wait_recv()
 
     def shifts(chunk):
-        return (1, 3) if chunk in FOLDED else (1, 3, 2)
+        return (1, 3) if chunk in FOLDED else (2, 1, 3)
 
     def xa_start(chunk, origin):
         block = bufs[chunk].at[index_of(origin, 0)]
@@ -326,14 +326,13 @@
             wins[group][b, REACH[group] : REACH[group] + rows, :] = key_norm(out, place, group)
         for group in order:
             for up in (True, False):
-                if group == 2:
+                if group != 2:
+                    halo(b, group, up).start()
+                elif b < 2:
 
                     @pl.when(x != (NX - 1 if up else 0))
                     def _(up=up):
                         halo(b, 2, up).start()
-
-                else:
-                    halo(b, group, up).start()
 
     for b in range(batch):
         key_step(b, 0, (2,))
@@ -344,12 +343,15 @@
 
         @pl.when(x == (NX - 1 if up else 0))
         def _(up=up):
-            for b in range(batch):
+            for b in range(2):
                 halo(b, 2, up).start()
 
     wk[:, 128:] = w01[...].reshape(wk.shape[0], 256)
     for b in range(batch):
         key_step(b, 128, (0, 1))
+        if 1 <= b < batch - 1:
+            for up in (True, False):
+                halo(b + 1, 2, up).start()
 
     all_blocks(2)
     wq[...] = wb[...].reshape(wq.shape)
@@ -454,7 +456,7 @@
     def pass_on(b):
         m_copy(b).wait_recv()
         mg[mine, b] = mboth[b, core] + mrecv[b]
-        for shift in range(1, tp):
+        for shift in (2, 1, 3):
             y_copy(b, shift).start()
 
     def attend_step(i, carry):

time: 54.4 us -> 52.2 us (0.960)
  Pallas kernels: 53.5 us -> 51.3 us
    pallas_call x1, Pallas kernels: 53.5 us -> 51.3 us  [body(): pl.pallas_call(functools.partial(layer_kernel, tp, batch, length), out_sh...]
where the time goes in v7:
time: 52.2 us; the launch traced here: 52 us
  Pallas kernels  51.3 us (98%)
  local copies, waits for them, and re-layouts  0.71 us (1%)
    pallas_call x1, Pallas kernels, body(): pl.pallas_call(functools.partial(layer_kernel, tp, batch, length), out_sh...  51.3 us

profile of v7, /device:TPU:1, one launch (start us, length us, event | category | flops | bytes accessed | tf_op | source)
XLA Modules:
  0.0 52.0 jit_solution(6015469734135430193)
XLA Ops:
  0.0 51.3 %layer.1 = bf16[4,128,256]{2,1,0:T(8,128)(2,1)S(1)} custom-call(bf16[4,128,1024]{2,1,0:T(8,128)(2,1)} %x_hbm.1, f32[1,1024]{1,0:T(1,128)} %bitcast.2, bf16[8,3,2,64]{3,2,1,0:T(2,128)(2,1)} %qw_hbm.1, bf16[8,3,2,64]{3,2,1,0:T(2,128)(2,1)} %kw_hbm.1, bf16[8,3,2,64]{3,2,1,0:T(2,128)(2,1)} %vw_hbm.1, bf16[2,8,64]{2,1,0:T(8,128)(2,1)} %bitcast.3, ...), custom_call_target="tpu_custom_call" | custom-call | tf_op jit(solution)/shard_map/layer/pallas_call | solution.py:530
  51.3 0.7 %copy.10 = bf16[4,128,256]{2,1,0:T(8,128)(2,1)} copy(bf16[4,128,256]{2,1,0:T(8,128)(2,1)S(1)} %layer.1) | data formatting | bytes 524288

commit v8 on v7

--- a/solution.py
+++ b/solution.py
@@ -306,8 +306,8 @@
             device_id_type=MESH,
         )
 
-    def halo_wait(b):
-        for group in (2, 1, 0):
+    def halo_wait(b, only=(2, 1, 0)):
+        for group in only:
             both = wins[group].at[b, pl.ds(0, 2 * REACH[group]), :]
             move(both, halo_send.at[group], halo_recv.at[b, group], at_chip(1)).wait_recv()
 
@@ -336,7 +336,6 @@
 
     for b in range(batch):
         key_step(b, 0, (2,))
-    all_blocks(1)
     sent_all(2)
 
     for up in (True, False):
@@ -346,6 +345,7 @@
             for b in range(2):
                 halo(b, 2, up).start()
 
+    all_blocks(1)
     wk[:, 128:] = w01[...].reshape(wk.shape[0], 256)
     for b in range(batch):
         key_step(b, 128, (0, 1))
@@ -437,9 +437,8 @@
             total, summed = total + part_total, summed + part_sum
         mboth[b] = merge(total, summed).reshape(2, length, 128)
 
-    def attend_block(b, block):
+    def attend_block(b, block, total, summed):
         begin = pl.multiple_of(block * length, length)
-        total, summed = wide_part(b, 2, begin, length)
         for part_total, part_sum in (wide_part(b, 1, begin, length), close_part(b, block)):
             total, summed = total + part_total, summed + part_sum
         mboth[b, block] = merge(total, summed)
@@ -473,11 +472,13 @@
 
     lax.fori_loop(0, batch - 1, attend_step, 0)
     last = batch - 1
-    halo_wait(last)
-    attend_block(last, other)
+    halo_wait(last, (2,))
+    far_parts = [wide_part(last, 2, pl.multiple_of(block * length, length), length) for block in (other, core)]
+    pass_on(last - 1)
+    halo_wait(last, (1, 0))
+    attend_block(last, other, *far_parts[0])
     m_copy(last).start()
-    pass_on(last - 1)
-    attend_block(last, core)
+    attend_block(last, core, *far_parts[1])
     pass_on(batch - 1)
     o_all.wait_recv()
 

time: 52.2 us -> 55.8 us (1.069)
  Pallas kernels: 51.3 us -> 55 us
    pallas_call x1, Pallas kernels: 51.3 us -> 55 us  [body(): pl.pallas_call(functools.partial(layer_kernel, tp, batch, length), out_sh...]
where the time goes in v8:
time: 55.8 us; the launch traced here: 55.7 us
  Pallas kernels  55 us (99%)
  local copies, waits for them, and re-layouts  0.71 us (1%)
    pallas_call x1, Pallas kernels, body(): pl.pallas_call(functools.partial(layer_kernel, tp, batch, length), out_sh...  55 us

profile of v8, /device:TPU:1, one launch (start us, length us, event | category | flops | bytes accessed | tf_op | source)
XLA Modules:
  0.0 55.7 jit_solution(13278554990957777642)
XLA Ops:
  0.0 55.0 %layer.1 = bf16[4,128,256]{2,1,0:T(8,128)(2,1)S(1)} custom-call(bf16[4,128,1024]{2,1,0:T(8,128)(2,1)} %x_hbm.1, f32[1,1024]{1,0:T(1,128)} %bitcast.2, bf16[8,3,2,64]{3,2,1,0:T(2,128)(2,1)} %qw_hbm.1, bf16[8,3,2,64]{3,2,1,0:T(2,128)(2,1)} %kw_hbm.1, bf16[8,3,2,64]{3,2,1,0:T(2,128)(2,1)} %vw_hbm.1, bf16[2,8,64]{2,1,0:T(8,128)(2,1)} %bitcast.3, ...), custom_call_target="tpu_custom_call" | custom-call | tf_op jit(solution)/shard_map/layer/pallas_call | solution.py:531
  55.0 0.7 %copy.10 = bf16[4,128,256]{2,1,0:T(8,128)(2,1)} copy(bf16[4,128,256]{2,1,0:T(8,128)(2,1)S(1)} %layer.1) | data formatting | bytes 524288

commit v9 on v8

--- a/solution.py
+++ b/solution.py
@@ -336,6 +336,7 @@
 
     for b in range(batch):
         key_step(b, 0, (2,))
+    all_blocks(1)
     sent_all(2)
 
     for up in (True, False):
@@ -345,7 +346,6 @@
             for b in range(2):
                 halo(b, 2, up).start()
 
-    all_blocks(1)
     wk[:, 128:] = w01[...].reshape(wk.shape[0], 256)
     for b in range(batch):
         key_step(b, 128, (0, 1))

time: 55.8 us -> 52.2 us (0.935)
  Pallas kernels: 55 us -> 51.3 us
    pallas_call x1, Pallas kernels: 55 us -> 51.3 us  [body(): pl.pallas_call(functools.partial(layer_kernel, tp, batch, length), out_sh...]
where the time goes in v9:
time: 52.2 us; the launch traced here: 52 us
  Pallas kernels  51.3 us (98%)
  local copies, waits for them, and re-layouts  0.71 us (1%)
    pallas_call x1, Pallas kernels, body(): pl.pallas_call(functools.partial(layer_kernel, tp, batch, length), out_sh...  51.3 us

profile of v9, /device:TPU:1, one launch (start us, length us, event | category | flops | bytes accessed | tf_op | source)
XLA Modules:
  0.0 52.0 jit_solution(6311911934822389164)
XLA Ops:
  0.0 51.3 %layer.1 = bf16[4,128,256]{2,1,0:T(8,128)(2,1)S(1)} custom-call(bf16[4,128,1024]{2,1,0:T(8,128)(2,1)} %x_hbm.1, f32[1,1024]{1,0:T(1,128)} %bitcast.2, bf16[8,3,2,64]{3,2,1,0:T(2,128)(2,1)} %qw_hbm.1, bf16[8,3,2,64]{3,2,1,0:T(2,128)(2,1)} %kw_hbm.1, bf16[8,3,2,64]{3,2,1,0:T(2,128)(2,1)} %vw_hbm.1, bf16[2,8,64]{2,1,0:T(8,128)(2,1)} %bitcast.3, ...), custom_call_target="tpu_custom_call" | custom-call | tf_op jit(solution)/shard_map/layer/pallas_call | solution.py:531
  51.3 0.7 %copy.10 = bf16[4,128,256]{2,1,0:T(8,128)(2,1)} copy(bf16[4,128,256]{2,1,0:T(8,128)(2,1)S(1)} %layer.1) | data formatting | bytes 524288
